TPU v7x, 128 devices: a whole 4x4x4 slice. The times are simulated.
128 devices in a mesh: ep: 64 (over z, y, x), tp: 2 (over core).
Axes of the slice: x: 4, y: 4, z: 4, core: 2. Of those that a mesh axis runs over, the one named last changes fastest.
Arguments:
- tokens: bfloat16 [1024, 2048], P('ep'), may hold values from -6 to 6
- state: float32 [1024, 8, 128, 128], P('ep', 'tp'), may hold values from -6 to 6
- mix_gain: float32 [2048], replicated, may hold values from 0.1 to 1.9
- moe_gain: float32 [2048], replicated, may hold values from 0.1 to 1.9
- head_gain: float32 [128], replicated, may hold values from 0.1 to 1.9
- w_forget: bfloat16 [2048, 1024], P(None, 'tp'), may hold values from -0.125 to 0.125
- w_query: bfloat16 [2048, 1024], P(None, 'tp'), may hold values from -0.125 to 0.125
- w_input: bfloat16 [2048, 1024], P(None, 'tp'), may hold values from -0.125 to 0.125
- w_outgate: bfloat16 [2048, 1024], P(None, 'tp'), may hold values from -0.125 to 0.125
- lower_bound: float32 [1024], P('tp'), may hold values from 0 to 0.9
- w_mix_out: bfloat16 [1024, 2048], P('tp'), may hold values from -0.1875 to 0.1875
- routes: int32 [1024, 6], P('ep'), may hold values from 0 to 63, all different within a row; in each aligned block of 16 rows (0 to 15, 16 to 31, ...) at most 4 rows name the same one
- route_scores: float32 [1024, 6], P('ep'), may hold values from 0.05 to 1
- expert_gate: bfloat16 [64, 2048, 512], P('ep', None, 'tp'), may hold values from -0.125 to 0.125
- expert_up: bfloat16 [64, 2048, 512], P('ep', None, 'tp'), may hold values from -0.125 to 0.125
- expert_down: bfloat16 [64, 512, 2048], P('ep', 'tp'), may hold values from -0.25 to 0.25
- shared_gate: bfloat16 [2048, 512], P(None, 'tp'), may hold values from -0.125 to 0.125
- shared_up: bfloat16 [2048, 512], P(None, 'tp'), may hold values from -0.125 to 0.125
- shared_down: bfloat16 [512, 2048], P('tp'), may hold values from -0.25 to 0.25
Outputs:
- layer_out: bfloat16 [1024, 2048], P('ep', 'tp')
- new_state: float32 [1024, 8, 128, 128], P('ep', 'tp')
Inputs may be any that keep to these rules, and one draw needn't show every extreme that they name: `routes`: each token names 6 different experts. Among the tokens of one index of ep no expert is named by more than 4 tokens, and in every draw some expert is named by exactly 4 tokens of some index of ep.
All inputs are finite; a program needn't handle non-finite values.
Results may differ from a plain program's by a relative error of at most 0.017.
Values may be sent and summed in bfloat16 or wider, within the bound.
A program may use at most 128 MiB of HBM per device.

v0:
```python
import jax
import jax.numpy as jnp
from jax import lax
from jax.sharding import PartitionSpec as P

epsilon = 1e-06
routed_scale = 2.5


def total_of_pieces(array, axis):
    tiles = lax.all_gather(array, axis).astype(jnp.float32)
    return tiles.sum(axis=0)


def cut_along(array, dim, devices):
    before, after = (array.shape[:dim], array.shape[dim + 1 :])
    return jnp.moveaxis(array.reshape(*before, devices, -1, *after), dim, 0)


def sent_and_summed(array, axis, dim):
    devices = lax.axis_size(axis)
    tiles = lax.all_to_all(cut_along(array, dim, devices), axis, 0, 0, tiled=True)
    return jnp.sum(tiles.astype(jnp.float32), axis=0)


def laid_out(tiles, dim):
    tiles = jnp.moveaxis(tiles, 0, dim)
    shape = tiles.shape
    return tiles.reshape(*shape[:dim], shape[dim] * shape[dim + 1], *shape[dim + 2 :])


def sent_to_all(array, axis):
    copies = jnp.broadcast_to(array, (lax.axis_size(axis), *array.shape))
    return lax.all_to_all(copies, axis, split_axis=0, concat_axis=0, tiled=True)


def gather_directly(array, axis, dim):
    return laid_out(sent_to_all(array, axis), dim)


def rms_scale(values, gain):
    return values * lax.rsqrt(jnp.mean(values * values, axis=-1, keepdims=True) + epsilon) * gain


def local(
    tokens,
    state,
    mix_gain,
    moe_gain,
    head_gain,
    w_forget,
    w_query,
    w_input,
    w_outgate,
    lower_bound,
    w_mix_out,
    routes,
    route_scores,
    expert_gate,
    expert_up,
    expert_down,
    shared_gate,
    shared_up,
    shared_down,
):
    seqs_here = tokens.shape[0]
    heads_here = state.shape[1]
    key_width = state.shape[2]
    value_width = state.shape[3]
    tokens_wide = tokens.astype(jnp.float32)
    normed = rms_scale(tokens_wide, mix_gain).astype(jnp.bfloat16)
    forget_pre = jnp.dot(normed, w_forget, preferred_element_type=jnp.float32).reshape(
        seqs_here, heads_here, key_width
    )
    query = jax.nn.silu(jnp.dot(normed, w_query, preferred_element_type=jnp.float32)).reshape(
        seqs_here, heads_here, key_width
    )
    input_val = jnp.dot(normed, w_input, preferred_element_type=jnp.float32).reshape(
        seqs_here, heads_here, value_width
    )
    gate_pre = jnp.dot(normed, w_outgate, preferred_element_type=jnp.float32).reshape(
        seqs_here, heads_here, value_width
    )
    bound_rows = lower_bound.reshape(heads_here, key_width)
    forget = bound_rows + (1.0 - bound_rows) * jax.nn.sigmoid(forget_pre)
    key_gate = (1.0 - bound_rows) * jax.nn.sigmoid(-forget_pre)
    new_state = forget[..., None] * state + key_gate[..., None] * input_val[:, :, None, :]
    readout = jnp.einsum("shkv,shk->shv", new_state, query)
    gated_out = (rms_scale(readout, head_gain) * jax.nn.silu(gate_pre)).astype(jnp.bfloat16)
    gated_out = gated_out.reshape(seqs_here, heads_here * value_width)
    partial_value = jnp.dot(gated_out, w_mix_out, preferred_element_type=jnp.float32)
    mixer_out = (
        total_of_pieces(partial_value.astype(jnp.bfloat16), "tp")
        .astype(jnp.float32)
        .astype(jnp.bfloat16)
    )
    residual = tokens_wide + mixer_out.astype(jnp.float32)
    moe_rows = rms_scale(residual, moe_gain).astype(jnp.bfloat16)
    full_width = moe_rows.shape[1]
    half_width = full_width // 2
    tp_index = lax.axis_index("tp")
    shared_hidden = (
        jax.nn.silu(jnp.dot(moe_rows, shared_gate, preferred_element_type=jnp.float32))
        * jnp.dot(moe_rows, shared_up, preferred_element_type=jnp.float32)
    ).astype(jnp.bfloat16)
    shared_part = jnp.dot(shared_hidden, shared_down, preferred_element_type=jnp.float32)
    shared_out = sent_and_summed(shared_part.astype(jnp.bfloat16), "tp", 1).astype(jnp.bfloat16)
    top_count = routes.shape[1]
    experts_all = expert_gate.shape[0] * lax.axis_size("ep")
    capacity = max(2, min(seqs_here, seqs_here * top_count * 3 // experts_all))
    flat_routes = routes.reshape(-1)
    onehot = (flat_routes[:, None] == jnp.arange(experts_all, dtype=jnp.int32)[None, :]).astype(
        jnp.int32
    )
    earlier = jnp.cumsum(onehot, axis=0) - onehot
    slot_rank = jnp.sum(earlier * onehot, axis=1)
    slot_index = flat_routes * capacity + slot_rank
    placing = (
        slot_index[None, :] == jnp.arange(experts_all * capacity, dtype=jnp.int32)[:, None]
    ).astype(jnp.int32)
    placing = (
        placing.reshape(experts_all * capacity, seqs_here, top_count)
        .sum(axis=2)
        .astype(jnp.bfloat16)
    )
    own_columns = lax.dynamic_slice_in_dim(moe_rows, tp_index * half_width, half_width, 1)
    outgoing = jnp.dot(placing, own_columns, preferred_element_type=jnp.float32).astype(
        jnp.bfloat16
    )
    outgoing = outgoing.reshape(experts_all, capacity, half_width)
    arrived_half = lax.all_to_all(outgoing, "ep", split_axis=0, concat_axis=1, tiled=True)
    arrived = gather_directly(arrived_half, "tp", 2)
    gate_act = jnp.einsum("esd,edf->esf", arrived, expert_gate, preferred_element_type=jnp.float32)
    up_act = jnp.einsum("esd,edf->esf", arrived, expert_up, preferred_element_type=jnp.float32)
    expert_hidden = (jax.nn.silu(gate_act) * up_act).astype(jnp.bfloat16)
    expert_part = jnp.einsum(
        "esf,efd->esd", expert_hidden, expert_down, preferred_element_type=jnp.float32
    )
    expert_half = sent_and_summed(expert_part.astype(jnp.bfloat16), "tp", 2).astype(jnp.bfloat16)
    returned = lax.all_to_all(expert_half, "ep", split_axis=1, concat_axis=0, tiled=True)
    pair_out = returned.reshape(experts_all * capacity, half_width)[slot_index].astype(jnp.float32)
    weights = route_scores / jnp.sum(route_scores, axis=-1, keepdims=True) * routed_scale
    routed = jnp.sum(
        pair_out.reshape(seqs_here, top_count, half_width) * weights[:, :, None], axis=1
    )
    residual_half = lax.dynamic_slice_in_dim(residual, tp_index * half_width, half_width, 1)
    layer_out = (residual_half + routed + shared_out.astype(jnp.float32)).astype(jnp.bfloat16)
    return (layer_out, new_state)


def solution(mesh):
    return jax.shard_map(
        local,
        mesh=mesh,
        in_specs=(
            P("ep", None),
            P("ep", "tp", None, None),
            P(),
            P(),
            P(),
            P(None, "tp"),
            P(None, "tp"),
            P(None, "tp"),
            P(None, "tp"),
            P("tp"),
            P("tp", None),
            P("ep", None),
            P("ep", None),
            P("ep", None, "tp"),
            P("ep", None, "tp"),
            P("ep", "tp", None),
            P(None, "tp"),
            P(None, "tp"),
            P("tp", None),
        ),
        out_specs=(P("ep", "tp"), P("ep", "tp", None, None)),
        check_vma=False,
    )
```

profile of v0, /device:TPU:1, one launch (start us, length us, event | category | flops | bytes accessed | tf_op | source)
XLA Modules:
  0.0 101.0 jit_solution(3535734524625955052)
XLA Ops:
  1.8 2.1 %fusion.34 = f32[16,512]{1,0:T(8,128)S(1)} fusion(bf16[2048,512]{1,0:T(8,128)(2,1)} %param.27, bf16[16,2048]{1,0:T(8,128)(2,1)} %param.19, f32[2048]{0:T(1024)} %param.21, f32[16]{0:T(128)S(1)} %add_rsqrt_fusion.2), kind=kOutput, calls=%fused_computation.71 | convolution fusion | flops 33685504 | bytes 2203712 | tf_op jit(solution)/shard_map/dot_general | solution.py:81
  3.9 2.0 %fusion.38 = f32[16,512]{1,0:T(8,128)S(1)} fusion(bf16[2048,512]{1,0:T(8,128)(2,1)} %param.26, bf16[16,2048]{1,0:T(8,128)(2,1)S(1)} %copy-done.2, f32[2048]{0:T(1024)S(1)} %copy-done.4, f32[16]{0:T(128)S(1)} %add_rsqrt_fusion.2), kind=kOutput, calls=%fused_computation.73 | convolution fusion | flops 33685504 | bytes 2203712 | tf_op jit(solution)/shard_map/dot_general | solution.py:78
  6.0 2.0 %add_divide_fusion.1 = (f32[16,512]{1,0:T(8,128)S(1)}, f32[16,512]{1,0:T(8,128)S(1)}) fusion(bf16[2048,512]{1,0:T(8,128)(2,1)} %param.24, bf16[16,2048]{1,0:T(8,128)(2,1)S(1)} %copy-done.2, f32[2048]{0:T(1024)S(1)} %copy-done.4, f32[16]{0:T(128)S(1)} %add_rsqrt_fusion.2), kind=kOutput, calls=%fused_computation.45 | convolution fusion | flops 33726464 | bytes 2236480 | tf_op jit(solution)/shard_map/dot_general | solution.py:72
  8.1 2.0 %divide_multiply_fusion.1 = f32[16,512]{1,0:T(8,128)S(1)} fusion(bf16[2048,512]{1,0:T(8,128)(2,1)} %param.25, bf16[16,2048]{1,0:T(8,128)(2,1)S(1)} %copy-done.2, f32[2048]{0:T(1024)S(1)} %copy-done.4, f32[16]{0:T(128)S(1)} %add_rsqrt_fusion.2), kind=kOutput, calls=%fused_computation.42 | convolution fusion | flops 33718272 | bytes 2203712 | tf_op jit(solution)/shard_map/dot_general | solution.py:75
  10.2 4.4 %multiply_add_fusion = f32[16,4,128,128]{3,2,1,0:T(8,128)S(1)} fusion(f32[16,4,128,128]{3,2,1,0:T(8,128)} %param.20, f32[16,4,128]{2,1,0:T(4,128)S(1)} %mul.181, f32[16,4,128]{2,1,0:T(4,128)S(1)} %bitcast.81, f32[16,4,128]{2,1,0:T(4,128)S(1)} %bitcast.80), kind=kLoop, calls=%fused_computation.1 | loop fusion | flops 3145728 | bytes 8486912 | tf_op jit(solution)/shard_map/add | solution.py:87
  15.2 1.3 %copy-done.1 = f32[16,4,128,128]{3,2,1,0:T(8,128)} copy-done((f32[16,4,128,128]{3,2,1,0:T(8,128)}, f32[16,4,128,128]{3,2,1,0:T(8,128)S(1)}, u32[]{:S(2)}) %copy-start.1) | copy-done | bytes 4194328
  17.2 2.9 %all-gather = bf16[32,2048]{1,0:T(8,128)(2,1)S(1)} all-gather(bf16[16,2048]{1,0:T(8,128)(2,1)S(1)} %convolution_convert_fusion.2), channel_id=2, replica_groups=mesh['ep'=64,'tp'=2] {'tp'}, dimensions={0}, use_global_device_ids=true | all-gather | bytes 196608 | tf_op jit(solution)/shard_map/all_gather | solution.py:11
  22.6 11.4 %all-to-all-start = ((bf16[64,4,1024]{2,1,0:T(4,128)(2,1)}), bf16[64,4,1024]{2,1,0:T(4,128)(2,1)S(1)}, u32[]{:S(2)}, u32[]{:S(2)}) async-start(bf16[64,4,1024]{2,1,0:T(4,128)(2,1)} %reshape.186), calls=%async_computation | async-start | bytes 1048576 | tf_op jit(solution)/shard_map/all_to_all | solution.py:131
  34.0 1.5 %fusion.45 = f32[16,256]{1,0:T(8,128)S(1)} fusion(bf16[16,2048]{1,0:T(8,128)(2,1)S(1)} %multiply_convert_fusion, bf16[2048,256]{1,0:T(8,128)(2,1)} %param.35), kind=kOutput, calls=%fused_computation.77 | convolution fusion | flops 16777216 | bytes 1130496 | tf_op jit(solution)/shard_map/dot_general | solution.py:103
  35.4 2.3 %convolution_convert_fusion.1 = bf16[16,2048]{1,0:T(8,128)(2,1)S(1)} fusion(bf16[256,2048]{1,0:T(8,128)(2,1)} %param.37, bf16[16,2048]{1,0:T(8,128)(2,1)S(1)} %multiply_convert_fusion, bf16[2048,256]{1,0:T(8,128)(2,1)} %param.36, f32[16,256]{1,0:T(8,128)S(1)} %fusion.45), kind=kOutput, calls=%fused_computation.3 | convolution fusion | flops 33611776 | bytes 2244608 | tf_op jit(solution)/shard_map/dot_general | solution.py:106
  38.5 8.0 %all-to-all-done = bf16[64,4,1024]{2,1,0:T(4,128)(2,1)S(1)} async-done(((bf16[64,4,1024]{2,1,0:T(4,128)(2,1)}), bf16[64,4,1024]{2,1,0:T(4,128)(2,1)S(1)}, u32[]{:S(2)}, u32[]{:S(2)}) %all-to-all-start) | async-done | bytes 524320 | tf_op jit(solution)/shard_map/all_to_all | solution.py:131
  46.8 6.2 %all_to_all.36 = bf16[2,1,256,1024]{2,3,1,0:T(8,128)(2,1)S(1)} all-to-all(bf16[2,1,256,1024]{2,3,1,0:T(8,128)(2,1)S(1)} %broadcast_in_dim.2), channel_id=1, replica_groups=mesh['ep'=64,'tp'=2] {'tp'}, dimensions={0} | all-to-all | bytes 2097152 | tf_op jit(solution)/shard_map/all_to_all | solution.py:34
  53.0 1.2 %fusion.5 = f32[256,256]{1,0:T(8,128)} fusion(bf16[256,2048]{0,1:T(8,128)(2,1)S(1)} %bitcast.72, bf16[1,2048,256]{2,1,0:T(8,128)(2,1)S(1)} %copy-done.3), kind=kOutput, calls=%fused_computation.12 | convolution fusion | flops 268435456 | bytes 2359296 | tf_op jit(solution)/shard_map/esd,edf->esf/dot_general | solution.py:133
  54.2 3.9 %convolution_convert_fusion = bf16[256,2048]{1,0:T(8,128)(2,1)} fusion(bf16[256,2048]{0,1:T(8,128)(2,1)S(1)} %bitcast.73, bf16[1,256,2048]{2,1,0:T(8,128)(2,1)} %param.34, bf16[1,2048,256]{2,1,0:T(8,128)(2,1)} %param.33, f32[256,256]{1,0:T(8,128)} %fusion.5), kind=kOutput, calls=%fused_computation.2 | convolution fusion | flops 537788416 | bytes 4456448 | tf_op jit(solution)/shard_map/esf,efd->esd/dot_general | solution.py:136
  58.2 1.8 %reshape.191 = bf16[1,256,2,1024]{3,2,1,0:T(2,128)(2,1)S(1)} reshape(bf16[256,2048]{1,0:T(8,128)(2,1)} %convolution_convert_fusion) | data formatting | bytes 2097152 | tf_op jit(solution)/shard_map/reshape | solution.py:17
  60.3 4.6 %all_to_all.37 = bf16[2,1,256,1024]{3,2,1,0:T(8,128)(2,1)S(1)} all-to-all(bf16[2,1,256,1024]{3,2,1,0:T(8,128)(2,1)S(1)} %bitcast.74), channel_id=1, replica_groups=mesh['ep'=64,'tp'=2] {'tp'}, dimensions={0} | all-to-all | bytes 2097152 | tf_op jit(solution)/shard_map/all_to_all | solution.py:22
  64.8 3.7 %all-to-all-start.4 = ((bf16[2,16,1024]{2,1,0:T(8,128)(2,1)}), bf16[2,16,1024]{2,1,0:T(8,128)(2,1)S(1)}, u32[]{:S(2)}, u32[]{:S(2)}) async-start(bf16[2,16,1024]{2,1,0:T(8,128)(2,1)} %bitcast.61), calls=%async_computation.4 | async-start | bytes 131072 | tf_op jit(solution)/shard_map/all_to_all | solution.py:22
  69.6 1.9 %copy.68 = bf16[1,256,1024]{2,0,1:T(2,128)(2,1)S(1)} copy(bf16[1,256,1024]{2,1,0:T(8,128)(2,1)} %bitcast.75) | data formatting | bytes 1048576 | tf_op jit(solution)/shard_map/reduce_sum | solution.py:23
  72.0 4.5 %reduce.4 = bf16[256,1024]{1,0:T(8,128)(2,1)} reduce(bf16[256,1,1024]{2,1,0:T(2,128)(2,1)S(1)} %bitcast.71, bf16[]{:T(256)} %broadcast.159), dimensions={1}, to_apply=%bitcast.62.reduce_sub_computation | reduce | bytes 1048578
  76.5 2.2 %reshape.207 = bf16[64,2,2048]{2,1,0:T(2,128)(2,1)} reshape(bf16[256,1024]{1,0:T(8,128)(2,1)} %reduce.4) | data formatting | bytes 1048576
  78.7 4.6 %all-to-all-start.3 = ((bf16[64,2,2048]{2,1,0:T(2,128)(2,1)}), bf16[64,2,2048]{2,1,0:T(2,128)(2,1)S(1)}, u32[]{:S(2)}, u32[]{:S(2)}) async-start(bf16[64,2,2048]{2,1,0:T(2,128)(2,1)} %reshape.207), calls=%async_computation.3 | async-start | bytes 1048576 | tf_op jit(solution)/shard_map/all_to_all | solution.py:140
  83.5 12.6 %all-to-all-done.3 = bf16[64,2,2048]{2,1,0:T(2,128)(2,1)S(1)} async-done(((bf16[64,2,2048]{2,1,0:T(2,128)(2,1)}), bf16[64,2,2048]{2,1,0:T(2,128)(2,1)S(1)}, u32[]{:S(2)}, u32[]{:S(2)}) %all-to-all-start.3) | async-done | bytes 524320 | tf_op jit(solution)/shard_map/all_to_all | solution.py:140
  96.1 1.8 %reshape.208 = bf16[256,1,1024]{2,1,0:T(2,128)(2,1)} reshape(bf16[64,2,2048]{2,1,0:T(2,128)(2,1)S(1)} %all-to-all-done.3) | data formatting | bytes 1048576
  97.9 1.4 %copy.66 = bf16[1,256,1024]{2,1,0:T(8,128)(2,1)S(1)} copy(bf16[1,256,1024]{2,0,1:T(2,128)(2,1)} %bitcast.70) | data formatting | bytes 1048576
  (69 shorter events, 9.7 us)
Async XLA Ops:
  0.6 16.2 %copy-start = (bf16[512,2048]{1,0:T(8,128)(2,1)S(1)}, bf16[512,2048]{1,0:T(8,128)(2,1)}, u32[]{:S(2)}) copy-start(bf16[512,2048]{1,0:T(8,128)(2,1)} %param.29) | copy-start | bytes 6291460
  0.6 3.3 %copy-start.2 = (bf16[16,2048]{1,0:T(8,128)(2,1)S(1)}, bf16[16,2048]{1,0:T(8,128)(2,1)}, u32[]{:S(2)}) copy-start(bf16[16,2048]{1,0:T(8,128)(2,1)} %param.19) | copy-start | bytes 196612
  0.7 3.2 %copy-start.4 = (f32[2048]{0:T(1024)S(1)}, f32[2048]{0:T(1024)}, u32[]{:S(2)}) copy-start(f32[2048]{0:T(1024)} %param.21) | copy-start | bytes 24580
  3.9 4.1 %copy-start.7 = (f32[512]{0:T(512)S(1)}, f32[512]{0:T(512)}, u32[]{:S(2)}) copy-start(f32[512]{0:T(512)} %param.28) | copy-start | bytes 6148
  14.6 2.0 %copy-start.1 = (f32[16,4,128,128]{3,2,1,0:T(8,128)}, f32[16,4,128,128]{3,2,1,0:T(8,128)S(1)}, u32[]{:S(2)}) copy-start(f32[16,4,128,128]{3,2,1,0:T(8,128)S(1)} %multiply_add_fusion) | copy-start | bytes 12582916
  14.6 2.1 %copy-start.9 = (f32[128]{0:T(128)S(1)}, f32[128]{0:T(128)}, u32[]{:S(2)}) copy-start(f32[128]{0:T(128)} %param.23) | copy-start | bytes 1540
  16.6 3.7 %copy-start.8 = (s32[16,6]{0,1:T(8,128)S(1)}, s32[16,6]{0,1:T(8,128)}, u32[]{:S(2)}) copy-start(s32[16,6]{0,1:T(8,128)} %param.30) | copy-start | bytes 1156
  16.6 4.6 %copy-start.6 = (f32[2048]{0:T(1024)S(1)}, f32[2048]{0:T(1024)}, u32[]{:S(2)}) copy-start(f32[2048]{0:T(1024)} %param.22) | copy-start | bytes 24580
  22.6 15.8 %copy-start.5 = (f32[16,6]{0,1:T(8,128)S(1)}, f32[16,6]{0,1:T(8,128)}, u32[]{:S(2)}) copy-start(f32[16,6]{0,1:T(8,128)} %param.31) | copy-start | bytes 1156
  22.6 23.8 %all-to-all-start = ((bf16[64,4,1024]{2,1,0:T(4,128)(2,1)}), bf16[64,4,1024]{2,1,0:T(4,128)(2,1)S(1)}, u32[]{:S(2)}, u32[]{:S(2)}) async-start(bf16[64,4,1024]{2,1,0:T(4,128)(2,1)} %reshape.186), calls=%async_computation | async-start | bytes 1048576 | tf_op jit(solution)/shard_map/all_to_all | solution.py:131
  46.7 6.3 %copy-start.3 = (bf16[1,2048,256]{2,1,0:T(8,128)(2,1)S(1)}, bf16[1,2048,256]{2,1,0:T(8,128)(2,1)}, u32[]{:S(2)}) copy-start(bf16[1,2048,256]{2,1,0:T(8,128)(2,1)} %param.32) | copy-start | bytes 3145732
  64.8 13.8 %all-to-all-start.4 = ((bf16[2,16,1024]{2,1,0:T(8,128)(2,1)}), bf16[2,16,1024]{2,1,0:T(8,128)(2,1)S(1)}, u32[]{:S(2)}, u32[]{:S(2)}) async-start(bf16[2,16,1024]{2,1,0:T(8,128)(2,1)} %bitcast.61), calls=%async_computation.4 | async-start | bytes 131072 | tf_op jit(solution)/shard_map/all_to_all | solution.py:22
  78.7 17.4 %all-to-all-start.3 = ((bf16[64,2,2048]{2,1,0:T(2,128)(2,1)}), bf16[64,2,2048]{2,1,0:T(2,128)(2,1)S(1)}, u32[]{:S(2)}, u32[]{:S(2)}) async-start(bf16[64,2,2048]{2,1,0:T(2,128)(2,1)} %reshape.207), calls=%async_computation.3 | async-start | bytes 1048576 | tf_op jit(solution)/shard_map/all_to_all | solution.py:140
where the time goes:
time: 102 us; the launch traced here: 101 us
  waiting for transfers between devices  20.6 us (20%)
  starting transfers between devices  19.7 us (19%)
  matrix products  18.4 us (18%)
  local copies, waits for them, and re-layouts  14.6 us (14%)
  blocking collectives  13.7 us (13%)
  other arithmetic  13 us (13%)
  between operations  1.02 us (1%)
    all_to_all x1, waiting for transfers between devices, local(): lax.all_to_all(expert_half, 'ep', split_axis=1, concat_axis=0, tiled=True)  12.6 us
    all_to_all x1, starting transfers between devices, local(): lax.all_to_all(outgoing, 'ep', split_axis=0, concat_axis=1, tiled=True)  11.4 us
    all_to_all x1, waiting for transfers between devices, local(): lax.all_to_all(outgoing, 'ep', split_axis=0, concat_axis=1, tiled=True)  7.96 us
    unnamed x27, local copies, waits for them, and re-layouts  7.34 us
    all_to_all x1, blocking collectives, sent_to_all(): return lax.all_to_all(copies, axis, split_axis=0, concat_axis=0, tiled=True)  6.2 us
    all_to_all x1, starting transfers between devices, local(): lax.all_to_all(expert_half, 'ep', split_axis=1, concat_axis=0, tiled=True)  4.63 us
    all_to_all x1, blocking collectives, sent_and_summed(): lax.all_to_all(cut_along(array, dim, devices), axis, 0, 0, tiled=True)  4.58 us
    unnamed x1, other arithmetic  4.5 us
  transfers between devices with their start and end apart: 3, of which 2 were waited for; matrix products, arithmetic and copies ran while one was open for 15% of the time, Pallas kernels for 0%

commit v1 on v0

--- a/solution.py
+++ b/solution.py
@@ -1,10 +1,248 @@
+import functools
+
 import jax
 import jax.numpy as jnp
 from jax import lax
+from jax.experimental import pallas as pl
+from jax.experimental.pallas import tpu as pltpu
 from jax.sharding import PartitionSpec as P
 
 epsilon = 1e-06
 routed_scale = 2.5
+MESH = pl.DeviceIdType.MESH
+bf16, f32, i32 = jnp.bfloat16, jnp.float32, jnp.int32
+
+
+def rms_scale(values, gain):
+    return values * lax.rsqrt(jnp.mean(values * values, axis=-1, keepdims=True) + epsilon) * gain
+
+
+def silu(v):
+    return v / (1.0 + jnp.exp(-v))
+
+
+def dot(a, b):
+    return jnp.dot(a, b, preferred_element_type=f32)
+
+
+def iota(shape, dim):
+    return lax.broadcasted_iota(i32, shape, dim)
+
+
+def toward(ep, off, sign):
+    z, y, x = ep // 16, (ep // 4) % 4, ep % 4
+    dz, dy, dx = off // 16, (off // 4) % 4, off % 4
+    if sign < 0:
+        dz, dy, dx = 4 - dz, 4 - dy, 4 - dx
+    return ((z + dz) % 4) * 16 + ((y + dy) % 4) * 4 + (x + dx) % 4
+
+
+def greet_all(ep, tp):
+    barrier = pltpu.get_barrier_semaphore()
+
+    def greet(i, c):
+        peer = toward(ep, i, 1)
+        for t in range(2):
+            pl.semaphore_signal(barrier, inc=1, device_id=(peer, t), device_id_type=MESH)
+        return c
+
+    lax.fori_loop(1, 64, greet, 0)
+    pl.semaphore_signal(barrier, inc=1, device_id=(ep, 1 - tp), device_id_type=MESH)
+
+
+def await_all():
+    pl.semaphore_wait(pltpu.get_barrier_semaphore(), 127)
+
+
+def route_tables(routes, scores, ep):
+    z, y, x = ep // 16, (ep // 4) % 4, ep % 4
+    weights = scores / jnp.sum(scores, axis=-1, keepdims=True) * routed_scale
+    rz = ((routes >> 4) - z) & 3
+    ry = (((routes >> 2) & 3) - y) & 3
+    rx = ((routes & 3) - x) & 3
+    rel = rz * 16 + ry * 4 + rx
+    lanes = iota((16, 64), 1)
+    named = jnp.zeros((16, 64), f32)
+    weight = jnp.zeros((16, 64), f32)
+    for k in range(6):
+        hit = rel[:, k : k + 1] == lanes
+        named = jnp.where(hit, 1.0, named)
+        weight = jnp.where(hit, weights[:, k : k + 1], weight)
+    earlier = (iota((16, 16), 1) < iota((16, 16), 0)).astype(bf16)
+    rank = dot(earlier, named.astype(bf16))
+    code = jnp.where(named > 0.5, rank + 1.0, 0.0)
+    return code, weight
+
+
+def place_rows(code, tp, place_ref):
+    spread = (iota((16, 128), 1) % 16 == iota((16, 128), 0)).astype(bf16)
+    codes = lax.dot_general(
+        code.astype(bf16), spread, (((0,), (0,)), ((), ())), preferred_element_type=f32
+    ).astype(bf16)
+    for b in range(4):
+        grow = (iota((256, 64), 0) // 16 + 16 * b == iota((256, 64), 1)).astype(bf16)
+        grown = dot(grow, codes)
+        row = iota((256, 128), 0) % 16
+        target = (2 * tp + row // 8 + 1).astype(f32)
+        fits = (grown == target) & (iota((256, 128), 1) // 16 == row % 8)
+        place_ref[pl.ds(256 * b, 256), :] = jnp.where(fits, 1.0, 0.0).astype(bf16)
+
+
+def combine_rows(code, weight, comb_ref):
+    both = jnp.concatenate([code, weight], axis=0).astype(bf16)
+    for n in range(8):
+        col = iota((64, 256), 1) + 256 * n
+        grow = (col // 32 == iota((64, 256), 0)).astype(bf16)
+        grown = dot(both, grow)
+        col = iota((16, 256), 1)
+        slot = ((col // 8) % 4 + 1).astype(f32)
+        value = jnp.where(grown[:16] == slot, grown[16:], 0.0)
+        for j in range(8):
+            comb_ref[pl.ds(16 * j, 16), pl.ds(256 * n, 256)] = jnp.where(
+                col % 8 == j, value, 0.0
+            ).astype(bf16)
+
+
+def moe_kernel(
+    rows_ref, routes_ref, scores_ref, gate_ref, up_ref, down_ref, out_ref,
+    gate_own, up_own, down_own, gate_par, up_par, down_par,
+    place, comb, send, recv, xs, ret, back,
+    load_sem, push_sem, pull_sem, go_send, go_recv, ret_send, ret_recv,
+):
+    ep, tp = lax.axis_index("ep"), lax.axis_index("tp")
+    partner = (ep, 1 - tp)
+    greet_all(ep, tp)
+    loads = [
+        pltpu.make_async_copy(src.at[0], dst, load_sem.at[i])
+        for i, (src, dst) in enumerate(((gate_ref, gate_own), (up_ref, up_own), (down_ref, down_own)))
+    ]
+    for copy in loads:
+        copy.start()
+    code, weight = route_tables(routes_ref[...], scores_ref[...], ep)
+    place_rows(code, tp, place)
+    combine_rows(code, weight, comb)
+    await_all()
+    pushes = [
+        pltpu.make_async_remote_copy(
+            src_ref=src.at[0], dst_ref=dst, send_sem=push_sem.at[i], recv_sem=pull_sem.at[i],
+            device_id=partner, device_id_type=MESH,
+        )
+        for i, (src, dst) in enumerate(((gate_ref, gate_par), (up_ref, up_par), (down_ref, down_par)))
+    ]
+    for copy in pushes:
+        copy.start()
+
+    rows = rows_ref[...]
+    stacked = jnp.concatenate([rows[:, 256 * j : 256 * (j + 1)] for j in range(8)], axis=0)
+
+    def go(i):
+        return pltpu.make_async_remote_copy(
+            src_ref=send.at[i], dst_ref=recv.at[i], send_sem=go_send, recv_sem=go_recv,
+            device_id=(toward(ep, i, 1), tp), device_id_type=MESH,
+        )
+
+    for b in range(4):
+        placed = dot(place[pl.ds(256 * b, 256), :], stacked).astype(bf16)
+        send[pl.ds(16 * b, 16)] = placed.reshape(16, 16, 256)
+
+        def start(i, c):
+            go(i).start()
+            return c
+
+        lax.fori_loop(max(1, 16 * b), 16 * b + 16, start, 0)
+    recv[0] = send[0]
+
+    def all_of(buf, n):
+        return buf.at[pl.ds(0, n)]
+
+    pltpu.make_async_remote_copy(
+        src_ref=all_of(send, 63), dst_ref=all_of(recv, 63), send_sem=go_send, recv_sem=go_recv,
+        device_id=partner, device_id_type=MESH,
+    ).wait()
+    for copy in loads:
+        copy.wait()
+    for copy in pushes:
+        copy.wait()
+
+    out_row, in_row = iota((256, 256), 0), iota((256, 256), 1)
+    sort = ((out_row // 32 == in_row % 8) & ((out_row // 2) % 16 == in_row // 16)
+            & (out_row % 2 == (in_row // 8) % 2)).astype(bf16)
+    unsort = ((in_row // 32 == out_row % 8) & ((in_row // 2) % 16 == out_row // 16)
+              & (in_row % 2 == (out_row // 8) % 2)).astype(bf16)
+    for b in range(4):
+        sorted_rows = dot(sort, recv[pl.ds(16 * b, 16)].reshape(256, 256)).astype(bf16)
+        for j in range(8):
+            xs[pl.ds(32 * b, 32), pl.ds(256 * j, 256)] = sorted_rows[32 * j : 32 * j + 32]
+    x = xs[...]
+    hidden_own = (silu(dot(x, gate_own[...])) * dot(x, up_own[...])).astype(bf16)
+    hidden_par = (silu(dot(x, gate_par[...])) * dot(x, up_par[...])).astype(bf16)
+    for n in range(8):
+        cols = pl.ds(256 * n, 256)
+        xs[:, cols] = (dot(hidden_own, down_own[:, cols]) + dot(hidden_par, down_par[:, cols])).astype(bf16)
+
+    def come(i, h):
+        return pltpu.make_async_remote_copy(
+            src_ref=ret.at[2 * i + h], dst_ref=back.at[2 * i + tp], send_sem=ret_send, recv_sem=ret_recv,
+            device_id=(toward(ep, i, -1), h), device_id_type=MESH,
+        )
+
+    for b in range(4):
+        tall = jnp.concatenate(
+            [
+                jnp.concatenate(
+                    [xs[pl.ds(32 * b, 32), pl.ds(128 * j + 1024 * h, 128)] for h in range(2)], axis=1
+                )
+                for j in range(8)
+            ],
+            axis=0,
+        )
+        turned = dot(unsort, tall).astype(bf16)
+        for i in range(16):
+            for h in range(2):
+                ret[2 * (16 * b + i) + h] = turned[16 * i : 16 * i + 16, 128 * h : 128 * h + 128]
+
+        def start_back(i, c):
+            for h in range(2):
+                come(i, h).start()
+            return c
+
+        lax.fori_loop(max(1, 16 * b), 16 * b + 16, start_back, 0)
+    pltpu.make_async_remote_copy(
+        src_ref=ret.at[1 - tp], dst_ref=back.at[tp], send_sem=ret_send, recv_sem=ret_recv,
+        device_id=partner, device_id_type=MESH,
+    ).start()
+    back[tp] = ret[tp]
+    pltpu.make_async_remote_copy(
+        src_ref=all_of(ret, 127), dst_ref=all_of(back, 127), send_sem=ret_send, recv_sem=ret_recv,
+        device_id=partner, device_id_type=MESH,
+    ).wait()
+    total = dot(comb[...], back[...].reshape(2048, 128))
+    for j in range(8):
+        out_ref[:, pl.ds(128 * j, 128)] = total[16 * j : 16 * j + 16]
+
+
+def moe(rows, routes, scores, gate, up, down):
+    vm = pl.BlockSpec(memory_space=pltpu.VMEM)
+    hbm = pl.BlockSpec(memory_space=pl.ANY)
+    dma = pltpu.SemaphoreType.DMA
+    return pl.pallas_call(
+        moe_kernel,
+        name="moe",
+        out_shape=jax.ShapeDtypeStruct((16, 1024), f32),
+        in_specs=[vm, vm, vm, hbm, hbm, hbm],
+        out_specs=vm,
+        scratch_shapes=[
+            pltpu.VMEM((2048, 256), bf16), pltpu.VMEM((2048, 256), bf16), pltpu.VMEM((256, 2048), bf16),
+            pltpu.VMEM((2048, 256), bf16), pltpu.VMEM((2048, 256), bf16), pltpu.VMEM((256, 2048), bf16),
+            pltpu.VMEM((1024, 128), bf16), pltpu.VMEM((128, 2048), bf16),
+            pltpu.VMEM((64, 16, 256), bf16), pltpu.VMEM((64, 16, 256), bf16), pltpu.VMEM((128, 2048), bf16),
+            pltpu.VMEM((128, 16, 128), bf16), pltpu.VMEM((128, 16, 128), bf16),
+            dma((3,)), dma((3,)), dma((3,)), dma, dma, dma, dma,
+        ],
+        compiler_params=pltpu.CompilerParams(
+            collective_id=0, has_side_effects=True, vmem_limit_bytes=48 << 20
+        ),
+    )(rows, routes, scores, gate, up, down)
 
 
 def total_of_pieces(array, axis):
@@ -36,10 +274,6 @@
 
 def gather_directly(array, axis, dim):
     return laid_out(sent_to_all(array, axis), dim)
-
-
-def rms_scale(values, gain):
-    return values * lax.rsqrt(jnp.mean(values * values, axis=-1, keepdims=True) + epsilon) * gain
 
 
 def local(
@@ -105,44 +339,7 @@
     ).astype(jnp.bfloat16)
     shared_part = jnp.dot(shared_hidden, shared_down, preferred_element_type=jnp.float32)
     shared_out = sent_and_summed(shared_part.astype(jnp.bfloat16), "tp", 1).astype(jnp.bfloat16)
-    top_count = routes.shape[1]
-    experts_all = expert_gate.shape[0] * lax.axis_size("ep")
-    capacity = max(2, min(seqs_here, seqs_here * top_count * 3 // experts_all))
-    flat_routes = routes.reshape(-1)
-    onehot = (flat_routes[:, None] == jnp.arange(experts_all, dtype=jnp.int32)[None, :]).astype(
-        jnp.int32
-    )
-    earlier = jnp.cumsum(onehot, axis=0) - onehot
-    slot_rank = jnp.sum(earlier * onehot, axis=1)
-    slot_index = flat_routes * capacity + slot_rank
-    placing = (
-        slot_index[None, :] == jnp.arange(experts_all * capacity, dtype=jnp.int32)[:, None]
-    ).astype(jnp.int32)
-    placing = (
-        placing.reshape(experts_all * capacity, seqs_here, top_count)
-        .sum(axis=2)
-        .astype(jnp.bfloat16)
-    )
-    own_columns = lax.dynamic_slice_in_dim(moe_rows, tp_index * half_width, half_width, 1)
-    outgoing = jnp.dot(placing, own_columns, preferred_element_type=jnp.float32).astype(
-        jnp.bfloat16
-    )
-    outgoing = outgoing.reshape(experts_all, capacity, half_width)
-    arrived_half = lax.all_to_all(outgoing, "ep", split_axis=0, concat_axis=1, tiled=True)
-    arrived = gather_directly(arrived_half, "tp", 2)
-    gate_act = jnp.einsum("esd,edf->esf", arrived, expert_gate, preferred_element_type=jnp.float32)
-    up_act = jnp.einsum("esd,edf->esf", arrived, expert_up, preferred_element_type=jnp.float32)
-    expert_hidden = (jax.nn.silu(gate_act) * up_act).astype(jnp.bfloat16)
-    expert_part = jnp.einsum(
-        "esf,efd->esd", expert_hidden, expert_down, preferred_element_type=jnp.float32
-    )
-    expert_half = sent_and_summed(expert_part.astype(jnp.bfloat16), "tp", 2).astype(jnp.bfloat16)
-    returned = lax.all_to_all(expert_half, "ep", split_axis=1, concat_axis=0, tiled=True)
-    pair_out = returned.reshape(experts_all * capacity, half_width)[slot_index].astype(jnp.float32)
-    weights = route_scores / jnp.sum(route_scores, axis=-1, keepdims=True) * routed_scale
-    routed = jnp.sum(
-        pair_out.reshape(seqs_here, top_count, half_width) * weights[:, :, None], axis=1
-    )
+    routed = moe(moe_rows, routes, route_scores, expert_gate, expert_up, expert_down)
     residual_half = lax.dynamic_slice_in_dim(residual, tp_index * half_width, half_width, 1)
     layer_out = (residual_half + routed + shared_out.astype(jnp.float32)).astype(jnp.bfloat16)
     return (layer_out, new_state)

time: 102 us -> 64.6 us (0.63)
  Pallas kernels: 0 us -> 32.9 us
  waiting for transfers between devices: 20.6 us -> 0.01 us
  starting transfers between devices: 19.7 us -> 3.64 us
  blocking collectives: 13.7 us -> 2.92 us
  local copies, waits for them, and re-layouts: 14.6 us -> 5.73 us
  matrix products: 18.4 us -> 11.4 us
  other arithmetic: 13 us -> 6.62 us
    pallas_call x0 -> x1, Pallas kernels: none -> 32.9 us  [moe(): pl.pallas_call(moe_kernel, name='moe', out_shape=jax.ShapeDtypeStruct((16...]
    all_to_all x2 -> x0, waiting for transfers between devices: 20.6 us -> none  [the longest x1 12.6 us: local(): lax.all_to_all(expert_half, 'ep', split_axis=1, concat_axis=0, tiled=True)]
    all_to_all x2 -> x0, starting transfers between devices: 16 us -> none  [the longest x1 11.4 us: local(): lax.all_to_all(outgoing, 'ep', split_axis=0, concat_axis=1, tiled=True)]
    all_to_all x2 -> x0, blocking collectives: 10.8 us -> none  [the longest x1 6.2 us: sent_to_all(): return lax.all_to_all(copies, axis, split_axis=0, concat_axis=0, tiled=True)]
    dot_general x3 -> x0, matrix products: 5.44 us -> none  [the longest x1 3.93 us: local(): jnp.einsum('esf,efd->esd', expert_hidden, expert_down, preferred_element_...]
    unnamed x1 -> x0, other arithmetic: 4.5 us -> none
    unnamed x27 -> x30, local copies, waits for them, and re-layouts: 7.34 us -> 5.01 us
    reshape x3 -> x1, local copies, waits for them, and re-layouts: 2.73 us -> 0.64 us  [cut_along(): return jnp.moveaxis(array.reshape(*before, devices, -1, *after), dim, 0)]
  transfers between devices with their start and end apart: 3 -> 1, of which waited for: 2 -> 0; matrix products, arithmetic and copies ran while one was open for 15% -> 0% of each run, Pallas kernels for 0% -> 51%
where the time goes in v1:
time: 64.6 us; the launch traced here: 64.1 us
  Pallas kernels  32.9 us (51%)
  matrix products  11.4 us (18%)
  other arithmetic  6.62 us (10%)
  local copies, waits for them, and re-layouts  5.73 us (9%)
  starting transfers between devices  3.64 us (6%)
  blocking collectives  2.92 us (5%)
  between operations  0.9 us (1%)
    pallas_call x1, Pallas kernels, moe(): pl.pallas_call(moe_kernel, name='moe', out_shape=jax.ShapeDtypeStruct((16...  32.9 us
    unnamed x30, local copies, waits for them, and re-layouts  5.01 us
    add x1, other arithmetic, local(): forget[..., None] * state + key_gate[..., None] * input_val[:, :, None, :]  4.39 us
    all_to_all x1, starting transfers between devices, sent_and_summed(): lax.all_to_all(cut_along(array, dim, devices), axis, 0, 0, tiled=True)  3.64 us
    all_gather x1, blocking collectives, total_of_pieces(): tiles = lax.all_gather(array, axis).astype(jnp.float32)  2.92 us
    dot_general x1, matrix products, local(): jnp.dot(shared_hidden, shared_down, preferred_element_type=jnp.float32)  2.27 us
    dot_general x1, matrix products, local(): jnp.dot(normed, w_forget, preferred_element_type=jnp.float32)  2.1 us
    dot_general x1, matrix products, local(): jnp.dot(normed, w_query, preferred_element_type=jnp.float32)  2.03 us
  transfers between devices with their start and end apart: 1, of which 0 were waited for; matrix products, arithmetic and copies ran while one was open for 0% of the time, Pallas kernels for 51%

profile of v1, /device:TPU:1, one launch (start us, length us, event | category | flops | bytes accessed | tf_op | source)
XLA Modules:
  0.0 64.1 jit_solution(15360143307340827501)
XLA Ops:
  0.7 1.1 %fusion.1 = f32[16]{0:T(128)S(1)} fusion(bf16[16,2048]{1,0:T(8,128)(2,1)} %param.19), kind=kLoop, calls=%fused_computation.8 | loop fusion | flops 98288 | bytes 65600 | tf_op jit(solution)/shard_map/reduce_sum | solution.py:17
  1.8 2.1 %add_divide_fusion.1 = (f32[16,512]{1,0:T(8,128)S(1)}, f32[16,512]{1,0:T(8,128)S(1)}) fusion(bf16[2048,512]{1,0:T(8,128)(2,1)} %param.24, bf16[16,2048]{1,0:T(8,128)(2,1)} %param.19, f32[2048]{0:T(1024)} %param.21, f32[16]{0:T(128)S(1)} %add_rsqrt_fusion.2), kind=kOutput, calls=%fused_computation.21 | convolution fusion | flops 33726464 | bytes 2236480 | tf_op jit(solution)/shard_map/dot_general | solution.py:306
  4.0 2.0 %fusion.19 = f32[16,512]{1,0:T(8,128)S(1)} fusion(bf16[2048,512]{1,0:T(8,128)(2,1)} %param.26, bf16[16,2048]{1,0:T(8,128)(2,1)S(1)} %copy-done.5, f32[2048]{0:T(1024)S(1)} %copy-done.7, f32[16]{0:T(128)S(1)} %add_rsqrt_fusion.2), kind=kOutput, calls=%fused_computation.39 | convolution fusion | flops 33685504 | bytes 2203712 | tf_op jit(solution)/shard_map/dot_general | solution.py:312
  6.0 2.0 %divide_multiply_fusion.1 = f32[16,512]{1,0:T(8,128)S(1)} fusion(bf16[2048,512]{1,0:T(8,128)(2,1)} %param.25, bf16[16,2048]{1,0:T(8,128)(2,1)S(1)} %copy-done.5, f32[2048]{0:T(1024)S(1)} %copy-done.7, f32[16]{0:T(128)S(1)} %add_rsqrt_fusion.2), kind=kOutput, calls=%fused_computation.18 | convolution fusion | flops 33718272 | bytes 2203712 | tf_op jit(solution)/shard_map/dot_general | solution.py:309
  8.1 4.4 %multiply_add_fusion = f32[16,4,128,128]{3,2,1,0:T(8,128)S(1)} fusion(f32[16,4,128,128]{3,2,1,0:T(8,128)} %param.20, f32[16,4,128]{2,1,0:T(4,128)S(1)} %mul.134, f32[16,4,128]{2,1,0:T(4,128)S(1)} %bitcast.40, f32[16,4,128]{2,1,0:T(4,128)S(1)} %bitcast.39), kind=kLoop, calls=%fused_computation | loop fusion | flops 3145728 | bytes 8486912 | tf_op jit(solution)/shard_map/add | solution.py:321
  12.6 0.7 %fusion.25 = f32[16,4,1,128]{3,2,1,0:T(1,128)S(1)} fusion(f32[16,4,128,128]{3,2,1,0:T(8,128)S(1)} %multiply_add_fusion, f32[16,4,128,1]{2,3,1,0:T(1,128)S(1)} %bitcast.41), kind=kOutput, calls=%fused_computation.41 | convolution fusion | flops 2097152 | bytes 4259840 | tf_op jit(solution)/shard_map/shkv,shk->shv/dot_general | solution.py:322
  13.2 1.5 %copy-done.4 = f32[16,4,128,128]{3,2,1,0:T(8,128)} copy-done((f32[16,4,128,128]{3,2,1,0:T(8,128)}, f32[16,4,128,128]{3,2,1,0:T(8,128)S(1)}, u32[]{:S(2)}) %copy-start.4) | copy-done | bytes 4194328
  14.7 0.1 multiply_reduce_fusion.1
  14.8 0.9 %copy-done.6 = bf16[2048,512]{1,0:T(8,128)(2,1)S(1)} copy-done((bf16[2048,512]{1,0:T(8,128)(2,1)S(1)}, bf16[2048,512]{1,0:T(8,128)(2,1)}, u32[]{:S(2)}) %copy-start.6) | copy-done | bytes 2097176
  15.7 0.4 fusion.15
  16.1 0.1 fusion.5
  16.2 0.4 convolution_convert_fusion.1
  16.6 2.9 %all-gather = bf16[32,2048]{1,0:T(8,128)(2,1)S(1)} all-gather(bf16[16,2048]{1,0:T(8,128)(2,1)S(1)} %convolution_convert_fusion.1), channel_id=2, replica_groups=mesh['ep'=64,'tp'=2] {'tp'}, dimensions={0}, use_global_device_ids=true | all-gather | bytes 196608 | tf_op jit(solution)/shard_map/all_gather | solution.py:249
  19.6 0.1 convert_add_fusion
  19.7 0.1 multiply_convert_fusion.rows_ref
  19.8 1.5 %fusion.26 = f32[16,256]{1,0:T(8,128)S(1)} fusion(bf16[16,2048]{1,0:T(8,128)(2,1)S(1)} %multiply_convert_fusion.rows_ref, bf16[2048,256]{1,0:T(8,128)(2,1)} %param.35), kind=kOutput, calls=%fused_computation.42 | convolution fusion | flops 16777216 | bytes 1130496 | tf_op jit(solution)/shard_map/dot_general | solution.py:337
  21.4 2.3 %convolution_convert_fusion = bf16[16,2048]{1,0:T(8,128)(2,1)S(1)} fusion(bf16[256,2048]{1,0:T(8,128)(2,1)} %param.37, bf16[16,2048]{1,0:T(8,128)(2,1)S(1)} %multiply_convert_fusion.rows_ref, bf16[2048,256]{1,0:T(8,128)(2,1)} %param.36, f32[16,256]{1,0:T(8,128)S(1)} %fusion.26), kind=kOutput, calls=%fused_computation.1 | convolution fusion | flops 33611776 | bytes 2244608 | tf_op jit(solution)/shard_map/dot_general | solution.py:340
  23.6 0.6 %copy.35 = bf16[2,2,8,1024]{3,2,0,1:T(8,128)(2,1)} copy(bf16[2,2,8,1024]{3,2,1,0:T(8,128)(2,1)S(1)} %bitcast.38) | data formatting | bytes 131072 | tf_op jit(solution)/shard_map/reshape | solution.py:255
  24.3 3.6 %all-to-all-start = ((bf16[2,16,1024]{2,1,0:T(8,128)(2,1)}), bf16[2,16,1024]{2,1,0:T(8,128)(2,1)S(1)}, u32[]{:S(2)}, u32[]{:S(2)}) async-start(bf16[2,16,1024]{2,1,0:T(8,128)(2,1)} %bitcast.28), calls=%async_computation | async-start | bytes 131072 | tf_op jit(solution)/shard_map/all_to_all | solution.py:260
  28.0 0.1 copy.24.scores_ref
  28.1 1.2 %copy-done.2 = bf16[1,2048,256]{2,1,0:T(8,128)(2,1)S(1)} copy-done((bf16[1,2048,256]{2,1,0:T(8,128)(2,1)S(1)}, bf16[1,2048,256]{2,1,0:T(8,128)(2,1)}, u32[]{:S(2)}) %copy-start.2) | copy-done | bytes 1048600
  29.3 1.2 %copy-done.3 = bf16[1,256,2048]{2,1,0:T(8,128)(2,1)S(1)} copy-done((bf16[1,256,2048]{2,1,0:T(8,128)(2,1)S(1)}, bf16[1,256,2048]{2,1,0:T(8,128)(2,1)}, u32[]{:S(2)}) %copy-start.3) | copy-done | bytes 1048600
  30.5 32.9 %moe.1 = f32[16,1024]{1,0:T(8,128)S(1)} custom-call(bf16[16,2048]{1,0:T(8,128)(2,1)S(1)} %multiply_convert_fusion.rows_ref, s32[16,6]{1,0:T(8,128)S(1)} %copy.23.routes_ref, f32[16,6]{1,0:T(8,128)S(1)} %copy.24.scores_ref, bf16[1,2048,256]{2,1,0:T(8,128)(2,1)S(1)} %copy-done.1, bf16[1,2048,256]{2,1,0:T(8,128)(2,1)S(1)} %copy-done.2, ...), custom_call_target="tpu_custom_call" | custom-call | tf_op jit(solution)/shard_map/moe/pallas_call | solution.py:228
  63.4 0.6 add_convert_fusion
  (38 shorter events, 0.3 us)
Async XLA Ops:
  0.6 15.6 %copy-start = (bf16[512,2048]{1,0:T(8,128)(2,1)S(1)}, bf16[512,2048]{1,0:T(8,128)(2,1)}, u32[]{:S(2)}) copy-start(bf16[512,2048]{1,0:T(8,128)(2,1)} %param.29) | copy-start | bytes 6291460
  0.6 3.3 %copy-start.5 = (bf16[16,2048]{1,0:T(8,128)(2,1)S(1)}, bf16[16,2048]{1,0:T(8,128)(2,1)}, u32[]{:S(2)}) copy-start(bf16[16,2048]{1,0:T(8,128)(2,1)} %param.19) | copy-start | bytes 196612
  0.7 3.3 %copy-start.7 = (f32[2048]{0:T(1024)S(1)}, f32[2048]{0:T(1024)}, u32[]{:S(2)}) copy-start(f32[2048]{0:T(1024)} %param.21) | copy-start | bytes 24580
  0.7 3.3 %copy-start.9 = (f32[512]{0:T(512)S(1)}, f32[512]{0:T(512)}, u32[]{:S(2)}) copy-start(f32[512]{0:T(512)} %param.28) | copy-start | bytes 6148
  12.5 2.1 %copy-start.4 = (f32[16,4,128,128]{3,2,1,0:T(8,128)}, f32[16,4,128,128]{3,2,1,0:T(8,128)S(1)}, u32[]{:S(2)}) copy-start(f32[16,4,128,128]{3,2,1,0:T(8,128)S(1)} %multiply_add_fusion) | copy-start | bytes 12582916
  12.5 3.1 %copy-start.6 = (bf16[2048,512]{1,0:T(8,128)(2,1)S(1)}, bf16[2048,512]{1,0:T(8,128)(2,1)}, u32[]{:S(2)}) copy-start(bf16[2048,512]{1,0:T(8,128)(2,1)} %param.27) | copy-start | bytes 6291460
  14.7 1.4 %copy-start.12 = (f32[128]{0:T(128)S(1)}, f32[128]{0:T(128)}, u32[]{:S(2)}) copy-start(f32[128]{0:T(128)} %param.23) | copy-start | bytes 1540
  15.7 4.1 %copy-start.8 = (f32[2048]{0:T(1024)S(1)}, f32[2048]{0:T(1024)}, u32[]{:S(2)}) copy-start(f32[2048]{0:T(1024)} %param.22) | copy-start | bytes 24580
  19.5 8.4 %copy-start.10 = (s32[16,6]{0,1:T(8,128)S(1)}, s32[16,6]{0,1:T(8,128)}, u32[]{:S(2)}) copy-start(s32[16,6]{0,1:T(8,128)} %param.30) | copy-start | bytes 1156
  19.6 8.4 %copy-start.11 = (f32[16,6]{0,1:T(8,128)S(1)}, f32[16,6]{0,1:T(8,128)}, u32[]{:S(2)}) copy-start(f32[16,6]{0,1:T(8,128)} %param.31) | copy-start | bytes 1156
  19.6 8.5 %copy-start.1 = (bf16[1,2048,256]{2,1,0:T(8,128)(2,1)S(1)}, bf16[1,2048,256]{2,1,0:T(8,128)(2,1)}, u32[]{:S(2)}) copy-start(bf16[1,2048,256]{2,1,0:T(8,128)(2,1)} %gate_ref.1) | copy-start | bytes 3145732
  24.3 39.1 %all-to-all-start = ((bf16[2,16,1024]{2,1,0:T(8,128)(2,1)}), bf16[2,16,1024]{2,1,0:T(8,128)(2,1)S(1)}, u32[]{:S(2)}, u32[]{:S(2)}) async-start(bf16[2,16,1024]{2,1,0:T(8,128)(2,1)} %bitcast.28), calls=%async_computation | async-start | bytes 131072 | tf_op jit(solution)/shard_map/all_to_all | solution.py:260
  28.1 1.2 %copy-start.2 = (bf16[1,2048,256]{2,1,0:T(8,128)(2,1)S(1)}, bf16[1,2048,256]{2,1,0:T(8,128)(2,1)}, u32[]{:S(2)}) copy-start(bf16[1,2048,256]{2,1,0:T(8,128)(2,1)} %up_ref.1) | copy-start | bytes 3145732
  29.3 1.2 %copy-start.3 = (bf16[1,256,2048]{2,1,0:T(8,128)(2,1)S(1)}, bf16[1,256,2048]{2,1,0:T(8,128)(2,1)}, u32[]{:S(2)}) copy-start(bf16[1,256,2048]{2,1,0:T(8,128)(2,1)} %down_ref.1) | copy-start | bytes 3145732

commit v2 on v1

v2 whole, which is shorter than its diff:
```python
import functools

import jax
import jax.numpy as jnp
from jax import lax
from jax.experimental import pallas as pl
from jax.experimental.pallas import tpu as pltpu
from jax.sharding import PartitionSpec as P

epsilon = 1e-06
routed_scale = 2.5
MESH = pl.DeviceIdType.MESH
bf16, f32, i32 = jnp.bfloat16, jnp.float32, jnp.int32


def rms_scale(values, gain):
    return values * lax.rsqrt(jnp.mean(values * values, axis=-1, keepdims=True) + epsilon) * gain


def silu(v):
    return v / (1.0 + jnp.exp(-v))


def dot(a, b):
    return jnp.dot(a, b, preferred_element_type=f32)


def iota(shape, dim):
    return lax.broadcasted_iota(i32, shape, dim)


def toward(ep, off, sign):
    z, y, x = ep // 16, (ep // 4) % 4, ep % 4
    dz, dy, dx = off // 16, (off // 4) % 4, off % 4
    if sign < 0:
        dz, dy, dx = 4 - dz, 4 - dy, 4 - dx
    return ((z + dz) % 4) * 16 + ((y + dy) % 4) * 4 + (x + dx) % 4


def greet_all(ep, tp):
    barrier = pltpu.get_barrier_semaphore()

    def greet(i, c):
        peer = toward(ep, i, 1)
        for t in range(2):
            pl.semaphore_signal(barrier, inc=1, device_id=(peer, t), device_id_type=MESH)
        return c

    lax.fori_loop(1, 64, greet, 0)
    pl.semaphore_signal(barrier, inc=1, device_id=(ep, 1 - tp), device_id_type=MESH)


def await_all():
    pl.semaphore_wait(pltpu.get_barrier_semaphore(), 127)


def route_tables(routes, scores, ep):
    z, y, x = ep // 16, (ep // 4) % 4, ep % 4
    weights = scores / jnp.sum(scores, axis=0, keepdims=True) * routed_scale
    rz = ((routes >> 4) - z) & 3
    ry = (((routes >> 2) & 3) - y) & 3
    rx = ((routes & 3) - x) & 3
    rel = rz * 16 + ry * 4 + rx
    experts = iota((64, 16), 0)
    named = jnp.zeros((64, 16), f32)
    weight = jnp.zeros((64, 16), f32)
    for k in range(6):
        hit = rel[k : k + 1, :] == experts
        named = jnp.where(hit, 1.0, named)
        weight = jnp.where(hit, weights[k : k + 1, :], weight)
    earlier = (iota((16, 16), 0) < iota((16, 16), 1)).astype(bf16)
    rank = dot(named.astype(bf16), earlier)
    code = jnp.where(named > 0.5, rank + 1.0, 0.0)
    return code.astype(bf16), weight.astype(bf16)


def place_rows(code, tp, place_ref):
    spread = (iota((16, 128), 1) % 16 == iota((16, 128), 0)).astype(bf16)
    codes = dot(code, spread).astype(bf16)
    for b in range(4):
        grow = (iota((256, 64), 0) // 16 + 16 * b == iota((256, 64), 1)).astype(bf16)
        grown = dot(grow, codes)
        row = iota((256, 128), 0) % 16
        target = (2 * tp + row // 8 + 1).astype(f32)
        fits = (grown == target) & (iota((256, 128), 1) // 16 == row % 8)
        place_ref[pl.ds(256 * b, 256), :] = jnp.where(fits, 1.0, 0.0).astype(bf16)


def combine_rows(code, weight, comb_ref):
    both = jnp.concatenate([code, weight], axis=1)
    for n in range(8):
        col = iota((64, 256), 1) + 256 * n
        grow = (col // 32 == iota((64, 256), 0)).astype(bf16)
        grown = lax.dot_general(both, grow, (((0,), (0,)), ((), ())), preferred_element_type=f32)
        col = iota((16, 256), 1)
        slot = ((col // 8) % 4 + 1).astype(f32)
        value = jnp.where(grown[:16] == slot, grown[16:], 0.0)
        for j in range(8):
            comb_ref[pl.ds(16 * j, 16), pl.ds(256 * n, 256)] = jnp.where(
                col % 8 == j, value, 0.0
            ).astype(bf16)


def all_of(buf, n):
    return buf.at[pl.ds(0, n)]


def layer_kernel(
    tokens_hbm, state_hbm, mix_gain_hbm, moe_gain_hbm, head_gain_hbm, forget_hbm, query_hbm, input_hbm,
    outgate_hbm, bound_hbm, mix_out_hbm, routes_hbm, scores_hbm, gate_hbm, up_hbm, down_hbm,
    sgate_hbm, sup_hbm, sdown_hbm,
    out_ref, state_out,
    tokens_v, mix_gain_v, moe_gain_v, head_gain_v, bound_v, routes_v, scores_v,
    forget_w, query_w, input_w, outgate_w, state_v, mix_w, sgate_w, sup_w, sdown_w,
    gate_own, up_own, down_own, gate_par, up_par, down_par,
    mix_send, mix_recv, shared_send, shared_recv, residual_v,
    forget_t, key_t, input_h, place, comb, send, recv, xs, ret, back,
    load_sem, half_sem, state_sem, late_sem, push_sem, pull_sem, mix_sems, shared_sems, go_send, go_recv, ret_send, ret_recv,
):
    ep, tp = lax.axis_index("ep"), lax.axis_index("tp")
    partner = (ep, 1 - tp)

    def to_partner(src, dst, send_sem, recv_sem):
        return pltpu.make_async_remote_copy(
            src_ref=src, dst_ref=dst, send_sem=send_sem, recv_sem=recv_sem, device_id=partner, device_id_type=MESH
        )

    small = [
        pltpu.make_async_copy(src, dst, load_sem.at[i])
        for i, (src, dst) in enumerate(
            (
                (tokens_hbm, tokens_v), (mix_gain_hbm, mix_gain_v), (routes_hbm, routes_v), (scores_hbm, scores_v),
                (bound_hbm, bound_v), (head_gain_hbm, head_gain_v), (moe_gain_hbm, moe_gain_v),
            )
        )
    ]
    for copy in small:
        copy.start()
    halves = []
    for i, (src, dst) in enumerate(
        ((forget_hbm, forget_w), (query_hbm, query_w), (input_hbm, input_w), (outgate_hbm, outgate_w))
    ):
        for h in range(2):
            rows = pl.ds(1024 * h, 1024)
            halves.append(pltpu.make_async_copy(src.at[rows], dst.at[rows], half_sem.at[2 * i + h]))
            halves[-1].start()
    states = []
    for c in range(4):
        rows = pl.ds(4 * c, 4)
        states.append(pltpu.make_async_copy(state_hbm.at[rows], state_v.at[rows], state_sem.at[c]))
        states[-1].start()
    mix_load = pltpu.make_async_copy(mix_out_hbm, mix_w, late_sem.at[0])
    mix_load.start()
    greet_all(ep, tp)

    for copy in small:
        copy.wait()
    code, weight = route_tables(routes_v[...], scores_v[...], ep)
    tokens = tokens_v[...].astype(f32)
    normed = rms_scale(tokens, mix_gain_v[...]).astype(bf16)
    place_rows(code, tp, place)

    def project(i, w):
        halves[2 * i].wait()
        first = dot(normed[:, :1024], w[:1024])
        halves[2 * i + 1].wait()
        return first + dot(normed[:, 1024:], w[1024:])

    forget_pre = project(0, forget_w)
    bound = bound_v[...]
    forget = bound + (1.0 - bound) / (1.0 + jnp.exp(-forget_pre))
    key = (1.0 - bound) / (1.0 + jnp.exp(forget_pre))
    query = silu(project(1, query_w))
    seen = forget * query
    input_val = project(2, input_w)
    gate = silu(project(3, outgate_w))
    late = [
        pltpu.make_async_copy(src, dst, late_sem.at[1 + i])
        for i, (src, dst) in enumerate(
            (
                (sgate_hbm, sgate_w), (sup_hbm, sup_w), (sdown_hbm, sdown_w),
                (gate_hbm.at[0], gate_own), (up_hbm.at[0], up_own), (down_hbm.at[0], down_own),
            )
        )
    ]
    for copy in late:
        copy.start()
    heads = [slice(128 * h, 128 * h + 128) for h in range(4)]
    readout = [
        jnp.sum(key[:, at] * query[:, at], axis=-1, keepdims=True) * input_val[:, at] for at in heads
    ]
    row, block = iota((16, 512), 0), iota((16, 512), 1) // 128
    for c in range(4):
        states[c].wait()
        for h in range(4):
            tiled = jnp.concatenate([seen[:, heads[h]]] * 4, axis=1)
            spread = jnp.where(row == block + 4 * c, tiled, 0.0).astype(bf16)
            readout[h] += dot(spread, state_v[pl.ds(4 * c, 4), h].reshape(512, 128).astype(bf16))
    head_gain = head_gain_v[...]
    gated = jnp.concatenate(
        [rms_scale(readout[h], head_gain) * gate[:, heads[h]] for h in range(4)], axis=1
    ).astype(bf16)
    mix_load.wait()
    mix_send[...] = dot(gated, mix_w[...]).astype(bf16)
    await_all()
    mix_copy = to_partner(mix_send, mix_recv, mix_sems.at[0], mix_sems.at[1])
    mix_copy.start()
    pushes = [
        to_partner(src.at[0], dst, push_sem.at[i], pull_sem.at[i])
        for i, (src, dst) in enumerate(((gate_hbm, gate_par), (up_hbm, up_par), (down_hbm, down_par)))
    ]
    for copy in pushes:
        copy.start()
    mix_copy.wait()
    mixer = (mix_send[...].astype(f32) + mix_recv[...].astype(f32)).astype(bf16)
    residual = tokens + mixer.astype(f32)
    for h in range(2):
        residual_v[h] = residual[:, 1024 * h : 1024 * (h + 1)]
    rows = rms_scale(residual, moe_gain_v[...]).astype(bf16)
    stacked = jnp.concatenate([rows[:, 256 * j : 256 * (j + 1)] for j in range(8)], axis=0)

    def go(i):
        return pltpu.make_async_remote_copy(
            src_ref=send.at[i], dst_ref=recv.at[i], send_sem=go_send, recv_sem=go_recv,
            device_id=(toward(ep, i, 1), tp), device_id_type=MESH,
        )

    for b in range(4):
        placed = dot(place[pl.ds(256 * b, 256), :], stacked).astype(bf16)
        send[pl.ds(16 * b, 16)] = placed.reshape(16, 16, 256)

        def start(i, c):
            go(i).start()
            return c

        lax.fori_loop(max(1, 16 * b), 16 * b + 16, start, 0)
    recv[0] = send[0]

    for copy in late[:3]:
        copy.wait()
    shared_hidden = (silu(dot(rows, sgate_w[...])) * dot(rows, sup_w[...])).astype(bf16)
    shared_part = dot(shared_hidden, sdown_w[...]).astype(bf16)
    for h in range(2):
        shared_send[h] = shared_part[:, 1024 * h : 1024 * (h + 1)]
    shared_copy = to_partner(shared_send.at[1 - tp], shared_recv, shared_sems.at[0], shared_sems.at[1])
    shared_copy.start()
    combine_rows(code, weight, comb)
    for h in range(4):
        forget_t[h] = forget[:, heads[h]].T
        key_t[h] = key[:, heads[h]].T
        input_h[h] = input_val[:, heads[h]]

    def update(h, c):
        keep, add, value = forget_t[h], key_t[h], input_h[h]
        for s in range(16):
            state_out[s, h] = keep[:, s : s + 1] * state_v[s, h] + add[:, s : s + 1] * value[s : s + 1, :]
        return c

    lax.fori_loop(0, 4, update, 0)
    for copy in late[3:]:
        copy.wait()
    for copy in pushes:
        copy.wait()
    pltpu.make_async_remote_copy(
        src_ref=all_of(send, 63), dst_ref=all_of(recv, 63), send_sem=go_send, recv_sem=go_recv,
        device_id=partner, device_id_type=MESH,
    ).wait()

    out_row, in_row = iota((256, 256), 0), iota((256, 256), 1)
    sort = ((out_row // 32 == in_row % 8) & ((out_row // 2) % 16 == in_row // 16)
            & (out_row % 2 == (in_row // 8) % 2)).astype(bf16)
    unsort = ((in_row // 32 == out_row % 8) & ((in_row // 2) % 16 == out_row // 16)
              & (in_row % 2 == (out_row // 8) % 2)).astype(bf16)
    for b in range(4):
        sorted_rows = dot(sort, recv[pl.ds(16 * b, 16)].reshape(256, 256)).astype(bf16)
        for j in range(8):
            xs[pl.ds(32 * b, 32), pl.ds(256 * j, 256)] = sorted_rows[32 * j : 32 * j + 32]
    x = xs[...]
    hidden_own = (silu(dot(x, gate_own[...])) * dot(x, up_own[...])).astype(bf16)
    hidden_par = (silu(dot(x, gate_par[...])) * dot(x, up_par[...])).astype(bf16)
    for n in range(8):
        cols = pl.ds(256 * n, 256)
        xs[:, cols] = (dot(hidden_own, down_own[:, cols]) + dot(hidden_par, down_par[:, cols])).astype(bf16)

    def come(i, h):
        return pltpu.make_async_remote_copy(
            src_ref=ret.at[2 * i + h], dst_ref=back.at[2 * i + tp], send_sem=ret_send, recv_sem=ret_recv,
            device_id=(toward(ep, i, -1), h), device_id_type=MESH,
        )

    for b in range(4):
        tall = jnp.concatenate(
            [
                jnp.concatenate(
                    [xs[pl.ds(32 * b, 32), pl.ds(128 * j + 1024 * h, 128)] for h in range(2)], axis=1
                )
                for j in range(8)
            ],
            axis=0,
        )
        turned = dot(unsort, tall).astype(bf16)
        for i in range(16):
            for h in range(2):
                ret[2 * (16 * b + i) + h] = turned[16 * i : 16 * i + 16, 128 * h : 128 * h + 128]

        def start_back(i, c):
            for h in range(2):
                come(i, h).start()
            return c

        lax.fori_loop(max(1, 16 * b), 16 * b + 16, start_back, 0)
    to_partner(ret.at[1 - tp], back.at[tp], ret_send, ret_recv).start()
    back[tp] = ret[tp]
    shared_copy.wait()
    base = residual_v[tp] + (shared_send[tp].astype(f32) + shared_recv[...].astype(f32)).astype(bf16).astype(f32)
    to_partner(all_of(ret, 127), all_of(back, 127), ret_send, ret_recv).wait()
    total = dot(comb[...], back[...].reshape(2048, 128))
    for j in range(8):
        cols = slice(128 * j, 128 * (j + 1))
        out_ref[:, cols] = (base[:, cols] + total[16 * j : 16 * j + 16]).astype(bf16)


def local(
    tokens, state, mix_gain, moe_gain, head_gain, w_forget, w_query, w_input, w_outgate, lower_bound, w_mix_out,
    routes, route_scores, expert_gate, expert_up, expert_down, shared_gate, shared_up, shared_down,
):
    vm = pl.BlockSpec(memory_space=pltpu.VMEM)
    hbm = pl.BlockSpec(memory_space=pltpu.HBM)
    dma = pltpu.SemaphoreType.DMA

    def buf(*shape, dtype=bf16):
        return pltpu.VMEM(shape, dtype)

    return pl.pallas_call(
        layer_kernel,
        name="layer",
        out_shape=(jax.ShapeDtypeStruct((16, 1024), bf16), jax.ShapeDtypeStruct((16, 4, 128, 128), f32)),
        in_specs=[hbm] * 19,
        out_specs=(vm, vm),
        scratch_shapes=[
            buf(16, 2048), buf(1, 2048, dtype=f32), buf(1, 2048, dtype=f32), buf(1, 128, dtype=f32),
            buf(1, 512, dtype=f32), buf(6, 16, dtype=i32), buf(6, 16, dtype=f32),
            buf(2048, 512), buf(2048, 512), buf(2048, 512), buf(2048, 512), buf(16, 4, 128, 128, dtype=f32),
            buf(512, 2048), buf(2048, 256), buf(2048, 256), buf(256, 2048),
            buf(2048, 256), buf(2048, 256), buf(256, 2048), buf(2048, 256), buf(2048, 256), buf(256, 2048),
            buf(16, 2048), buf(16, 2048), buf(2, 16, 1024), buf(16, 1024), buf(2, 16, 1024, dtype=f32),
            buf(4, 128, 16, dtype=f32), buf(4, 128, 16, dtype=f32), buf(4, 16, 128, dtype=f32),
            buf(1024, 128), buf(128, 2048), buf(64, 16, 256), buf(64, 16, 256), buf(128, 2048),
            buf(128, 16, 128), buf(128, 16, 128),
            dma((7,)), dma((8,)), dma((4,)), dma((7,)), dma((3,)), dma((3,)), dma((2,)), dma((2,)), dma, dma, dma, dma,
        ],
        compiler_params=pltpu.CompilerParams(
            collective_id=0, has_side_effects=True, vmem_limit_bytes=56 << 20
        ),
    )(
        tokens, state, mix_gain.reshape(1, -1), moe_gain.reshape(1, -1), head_gain.reshape(1, -1),
        w_forget, w_query, w_input, w_outgate, lower_bound.reshape(1, -1), w_mix_out,
        routes.T, route_scores.T, expert_gate, expert_up, expert_down, shared_gate, shared_up, shared_down,
    )


def solution(mesh):
    return jax.shard_map(
        local,
        mesh=mesh,
        in_specs=(
            P("ep", None),
            P("ep", "tp", None, None),
            P(),
            P(),
            P(),
            P(None, "tp"),
            P(None, "tp"),
            P(None, "tp"),
            P(None, "tp"),
            P("tp"),
            P("tp", None),
            P("ep", None),
            P("ep", None),
            P("ep", None, "tp"),
            P("ep", None, "tp"),
            P("ep", "tp", None),
            P(None, "tp"),
            P(None, "tp"),
            P("tp", None),
        ),
        out_specs=(P("ep", "tp"), P("ep", "tp", None, None)),
        check_vma=False,
    )
```

time: 64.6 us -> 46.1 us (0.71)
  matrix products: 11.4 us -> 0 us
  other arithmetic: 6.62 us -> 0 us
  Pallas kernels: 32.9 us -> 39.1 us
  starting transfers between devices: 3.64 us -> 0 us
  blocking collectives: 2.92 us -> 0 us
    dot_general x8 -> x0, matrix products: 11.4 us -> none  [the longest x1 2.27 us: local(): jnp.dot(shared_hidden, shared_down, preferred_element_type=jnp.float32)]
    pallas_call x1, Pallas kernels: 32.9 us -> 39.1 us  [local(): pl.pallas_call(layer_kernel, name='layer', out_shape=(jax.ShapeDtypeStruc...]
    add x3 -> x0, other arithmetic: 4.54 us -> none  [the longest x1 4.39 us: local(): forget[..., None] * state + key_gate[..., None] * input_val[:, :, None, :]]
    all_to_all x1 -> x0, starting transfers between devices: 3.64 us -> none  [sent_and_summed(): lax.all_to_all(cut_along(array, dim, devices), axis, 0, 0, tiled=True)]
    all_gather x1 -> x0, blocking collectives: 2.92 us -> none  [total_of_pieces(): tiles = lax.all_gather(array, axis).astype(jnp.float32)]
    reduce_sum x4 -> x0, other arithmetic: 1.24 us -> none  [the longest x2 1.21 us: rms_scale(): jnp.mean(values * values, axis=-1, keepdims=True) + epsilon]
    unnamed x30 -> x2, local copies, waits for them, and re-layouts: 5.01 us -> 6.07 us
    convert_element_type x3 -> x0, other arithmetic: 0.81 us -> none  [the longest x1 0.63 us: local(): (residual_half + routed + shared_out.astype(jnp.float32)).astype(jnp.bflo...]
  transfers between devices with their start and end apart: 1 -> 0, of which waited for: 0 -> 0; matrix products, arithmetic and copies ran while one was open for 0% -> 0% of each run, Pallas kernels for 51% -> 0%
where the time goes in v2:
time: 46.1 us; the launch traced here: 45.9 us
  Pallas kernels  39.1 us (85%)
  local copies, waits for them, and re-layouts  6.07 us (13%)
  between operations  0.65 us (1%)
    pallas_call x1, Pallas kernels, local(): pl.pallas_call(layer_kernel, name='layer', out_shape=(jax.ShapeDtypeStruc...  39.1 us
    unnamed x2, local copies, waits for them, and re-layouts  6.07 us

profile of v2, /device:TPU:1, one launch (start us, length us, event | category | flops | bytes accessed | tf_op | source)
XLA Modules:
  0.0 45.9 jit_solution(667631375951339239)
XLA Ops:
  0.6 39.1 %layer.1 = (bf16[16,1024]{1,0:T(8,128)(2,1)}, f32[16,4,128,128]{3,2,1,0:T(8,128)}) custom-call(bf16[16,2048]{1,0:T(8,128)(2,1)} %tokens_hbm.1, f32[16,4,128,128]{3,2,1,0:T(8,128)} %state_hbm.1, f32[1,2048]{1,0:T(1,128)} %bitcast.6, f32[1,2048]{1,0:T(1,128)} %bitcast.7, f32[1,128]{1,0:T(1,128)} %bitcast.11, bf16[2048,512]{1,0:T(8,128)(2,1)} %forget_hbm.1, ...), custom_call_target="tpu_custom_call" | custom-call | tf_op jit(solution)/shard_map/layer/pallas_call | solution.py:334
  39.8 1.4 %copy.23 = bf16[16,1024]{1,0:T(8,128)(2,1)} copy(bf16[16,1024]{1,0:T(8,128)(2,1)} %get-tuple-element.4) | data formatting | bytes 65536
  41.2 4.7 %copy.24 = f32[16,4,128,128]{3,2,1,0:T(8,128)} copy(f32[16,4,128,128]{3,2,1,0:T(8,128)} %get-tuple-element.5) | data formatting | bytes 8388608

commit v3 on v2

--- a/solution.py
+++ b/solution.py
@@ -10,6 +10,7 @@
 epsilon = 1e-06
 routed_scale = 2.5
 MESH = pl.DeviceIdType.MESH
+vmem_all = 67043328
 bf16, f32, i32 = jnp.bfloat16, jnp.float32, jnp.int32
 
 
@@ -109,12 +110,12 @@
     tokens_hbm, state_hbm, mix_gain_hbm, moe_gain_hbm, head_gain_hbm, forget_hbm, query_hbm, input_hbm,
     outgate_hbm, bound_hbm, mix_out_hbm, routes_hbm, scores_hbm, gate_hbm, up_hbm, down_hbm,
     sgate_hbm, sup_hbm, sdown_hbm,
-    out_ref, state_out,
+    state_out, back, comb, base_out,
     tokens_v, mix_gain_v, moe_gain_v, head_gain_v, bound_v, routes_v, scores_v,
     forget_w, query_w, input_w, outgate_w, state_v, mix_w, sgate_w, sup_w, sdown_w,
     gate_own, up_own, down_own, gate_par, up_par, down_par,
     mix_send, mix_recv, shared_send, shared_recv, residual_v,
-    forget_t, key_t, input_h, place, comb, send, recv, xs, ret, back,
+    forget_t, key_t, input_h, place, send, recv, xs, ret,
     load_sem, half_sem, state_sem, late_sem, push_sem, pull_sem, mix_sems, shared_sems, go_send, go_recv, ret_send, ret_recv,
 ):
     ep, tp = lax.axis_index("ep"), lax.axis_index("tp")
@@ -312,12 +313,21 @@
     to_partner(ret.at[1 - tp], back.at[tp], ret_send, ret_recv).start()
     back[tp] = ret[tp]
     shared_copy.wait()
-    base = residual_v[tp] + (shared_send[tp].astype(f32) + shared_recv[...].astype(f32)).astype(bf16).astype(f32)
+    base_out[...] = residual_v[tp] + (shared_send[tp].astype(f32) + shared_recv[...].astype(f32)).astype(bf16).astype(f32)
     to_partner(all_of(ret, 127), all_of(back, 127), ret_send, ret_recv).wait()
-    total = dot(comb[...], back[...].reshape(2048, 128))
+
+
+def finish_kernel(state_ref, back_ref, comb_ref, base_ref, out_hbm, state_hbm, out_v, sems):
+    state_copy = pltpu.make_async_copy(state_ref, state_hbm, sems.at[0])
+    state_copy.start()
+    total = dot(comb_ref[...], back_ref[...].reshape(2048, 128))
     for j in range(8):
         cols = slice(128 * j, 128 * (j + 1))
-        out_ref[:, cols] = (base[:, cols] + total[16 * j : 16 * j + 16]).astype(bf16)
+        out_v[:, cols] = (base_ref[:, cols] + total[16 * j : 16 * j + 16]).astype(bf16)
+    out_copy = pltpu.make_async_copy(out_v, out_hbm, sems.at[1])
+    out_copy.start()
+    out_copy.wait()
+    state_copy.wait()
 
 
 def local(
@@ -331,12 +341,14 @@
     def buf(*shape, dtype=bf16):
         return pltpu.VMEM(shape, dtype)
 
-    return pl.pallas_call(
+    kept = pl.pallas_call(
         layer_kernel,
         name="layer",
-        out_shape=(jax.ShapeDtypeStruct((16, 1024), bf16), jax.ShapeDtypeStruct((16, 4, 128, 128), f32)),
+        out_shape=(
+            buf(16, 4, 128, 128, dtype=f32), buf(128, 16, 128), buf(128, 2048), buf(16, 1024, dtype=f32)
+        ),
         in_specs=[hbm] * 19,
-        out_specs=(vm, vm),
+        out_specs=(vm,) * 4,
         scratch_shapes=[
             buf(16, 2048), buf(1, 2048, dtype=f32), buf(1, 2048, dtype=f32), buf(1, 128, dtype=f32),
             buf(1, 512, dtype=f32), buf(6, 16, dtype=i32), buf(6, 16, dtype=f32),
@@ -345,18 +357,26 @@
             buf(2048, 256), buf(2048, 256), buf(256, 2048), buf(2048, 256), buf(2048, 256), buf(256, 2048),
             buf(16, 2048), buf(16, 2048), buf(2, 16, 1024), buf(16, 1024), buf(2, 16, 1024, dtype=f32),
             buf(4, 128, 16, dtype=f32), buf(4, 128, 16, dtype=f32), buf(4, 16, 128, dtype=f32),
-            buf(1024, 128), buf(128, 2048), buf(64, 16, 256), buf(64, 16, 256), buf(128, 2048),
-            buf(128, 16, 128), buf(128, 16, 128),
+            buf(1024, 128), buf(64, 16, 256), buf(64, 16, 256), buf(128, 2048), buf(128, 16, 128),
             dma((7,)), dma((8,)), dma((4,)), dma((7,)), dma((3,)), dma((3,)), dma((2,)), dma((2,)), dma, dma, dma, dma,
         ],
         compiler_params=pltpu.CompilerParams(
-            collective_id=0, has_side_effects=True, vmem_limit_bytes=56 << 20
+            collective_id=0, has_side_effects=True, vmem_limit_bytes=vmem_all - (5 << 20) - (160 << 10)
         ),
     )(
         tokens, state, mix_gain.reshape(1, -1), moe_gain.reshape(1, -1), head_gain.reshape(1, -1),
         w_forget, w_query, w_input, w_outgate, lower_bound.reshape(1, -1), w_mix_out,
         routes.T, route_scores.T, expert_gate, expert_up, expert_down, shared_gate, shared_up, shared_down,
     )
+    return pl.pallas_call(
+        finish_kernel,
+        name="finish",
+        out_shape=(jax.ShapeDtypeStruct((16, 1024), bf16), jax.ShapeDtypeStruct((16, 4, 128, 128), f32)),
+        in_specs=[vm] * 4,
+        out_specs=(hbm, hbm),
+        scratch_shapes=[buf(16, 1024), dma((2,))],
+        compiler_params=pltpu.CompilerParams(vmem_limit_bytes=8 << 20),
+    )(*kept)
 
 
 def solution(mesh):

time: 46.1 us -> 39.4 us (0.85)
  local copies, waits for them, and re-layouts: 6.07 us -> 0 us
    unnamed x2 -> x0, local copies, waits for them, and re-layouts: 6.07 us -> none
    pallas_call x1 -> x2, Pallas kernels: 39.1 us -> 38.7 us  [the longest x1 36.6 us: local(): pl.pallas_call(layer_kernel, name='layer', out_shape=(buf(16, 4, 128, 128...]
where the time goes in v3:
time: 39.4 us; the launch traced here: 39.3 us
  Pallas kernels  38.7 us (98%)
  between operations  0.65 us (2%)
    pallas_call x1, Pallas kernels, local(): pl.pallas_call(layer_kernel, name='layer', out_shape=(buf(16, 4, 128, 128...  36.6 us
    pallas_call x1, Pallas kernels, local(): pl.pallas_call(finish_kernel, name='finish', out_shape=(jax.ShapeDtypeStr...  2.03 us

profile of v3, /device:TPU:1, one launch (start us, length us, event | category | flops | bytes accessed | tf_op | source)
XLA Modules:
  0.0 39.3 jit_solution(2151164929394759496)
XLA Ops:
  0.6 36.6 %layer.1 = (f32[16,4,128,128]{3,2,1,0:T(8,128)S(1)}, bf16[128,16,128]{2,1,0:T(8,128)(2,1)S(1)}, bf16[128,2048]{1,0:T(8,128)(2,1)S(1)}, f32[16,1024]{1,0:T(8,128)S(1)}) custom-call(bf16[16,2048]{1,0:T(8,128)(2,1)} %tokens_hbm.1, f32[16,4,128,128]{3,2,1,0:T(8,128)} %state_hbm.1, f32[1,2048]{1,0:T(1,128)} %bitcast.6, f32[1,2048]{1,0:T(1,128)} %bitcast.7, ...), custom_call_target="tpu_custom_call" | custom-call | tf_op jit(solution)/shard_map/layer/pallas_call | solution.py:344
  37.3 2.0 %finish.1 = (bf16[16,1024]{1,0:T(8,128)(2,1)}, f32[16,4,128,128]{3,2,1,0:T(8,128)}) custom-call(f32[16,4,128,128]{3,2,1,0:T(8,128)S(1)} %get-tuple-element.6.state_ref, bf16[128,16,128]{2,1,0:T(8,128)(2,1)S(1)} %get-tuple-element.7.back_ref, bf16[128,2048]{1,0:T(8,128)(2,1)S(1)} %get-tuple-element.8.comb_ref, f32[16,1024]{1,0:T(8,128)S(1)} %get-tuple-element.9.base_ref), custom_call_target="tpu_custom_call" | custom-call | tf_op jit(solution)/shard_map/finish/pallas_call | solution.py:371

commit v4 on v3

--- a/solution.py
+++ b/solution.py
@@ -1,7 +1,6 @@
-import functools
-
 import jax
 import jax.numpy as jnp
+import numpy as np
 from jax import lax
 from jax.experimental import pallas as pl
 from jax.experimental.pallas import tpu as pltpu
@@ -30,24 +29,38 @@
     return lax.broadcasted_iota(i32, shape, dim)
 
 
-def toward(ep, off, sign):
-    z, y, x = ep // 16, (ep // 4) % 4, ep % 4
-    dz, dy, dx = off // 16, (off // 4) % 4, off % 4
-    if sign < 0:
-        dz, dy, dx = 4 - dz, 4 - dy, 4 - dx
-    return ((z + dz) % 4) * 16 + ((y + dy) % 4) * 4 + (x + dx) % 4
-
-
-def greet_all(ep, tp):
+def parts(off):
+    return off // 16, off // 4 % 4, off % 4
+
+
+def hops(off):
+    return sum(min(d, 4 - d) for d in parts(off))
+
+
+order = sorted(range(64), key=lambda off: (-hops(off), off * 37 % 64))
+
+
+class Peers:
+    def __init__(self, ep):
+        z, y, x = ep // 16, lax.rem(ep // 4, 4), lax.rem(ep, 4)
+        self.z = [lax.rem(z + d, 4) * 16 for d in range(4)]
+        self.y = [lax.rem(y + d, 4) * 4 for d in range(4)]
+        self.x = [lax.rem(x + d, 4) for d in range(4)]
+
+    def ahead(self, p):
+        dz, dy, dx = parts(order[p])
+        return self.z[dz] + self.y[dy] + self.x[dx]
+
+    def behind(self, p):
+        dz, dy, dx = parts(order[p])
+        return self.z[-dz % 4] + self.y[-dy % 4] + self.x[-dx % 4]
+
+
+def greet_all(ep, tp, peers):
     barrier = pltpu.get_barrier_semaphore()
-
-    def greet(i, c):
-        peer = toward(ep, i, 1)
+    for p in range(63):
         for t in range(2):
-            pl.semaphore_signal(barrier, inc=1, device_id=(peer, t), device_id_type=MESH)
-        return c
-
-    lax.fori_loop(1, 64, greet, 0)
+            pl.semaphore_signal(barrier, inc=1, device_id=(peers.ahead(p), t), device_id_type=MESH)
     pl.semaphore_signal(barrier, inc=1, device_id=(ep, 1 - tp), device_id_type=MESH)
 
 
@@ -55,14 +68,13 @@
     pl.semaphore_wait(pltpu.get_barrier_semaphore(), 127)
 
 
-def route_tables(routes, scores, ep):
+def route_tables(routes, scores, experts, ep):
     z, y, x = ep // 16, (ep // 4) % 4, ep % 4
     weights = scores / jnp.sum(scores, axis=0, keepdims=True) * routed_scale
     rz = ((routes >> 4) - z) & 3
     ry = (((routes >> 2) & 3) - y) & 3
     rx = ((routes & 3) - x) & 3
     rel = rz * 16 + ry * 4 + rx
-    experts = iota((64, 16), 0)
     named = jnp.zeros((64, 16), f32)
     weight = jnp.zeros((64, 16), f32)
     for k in range(6):
@@ -109,9 +121,9 @@
 def layer_kernel(
     tokens_hbm, state_hbm, mix_gain_hbm, moe_gain_hbm, head_gain_hbm, forget_hbm, query_hbm, input_hbm,
     outgate_hbm, bound_hbm, mix_out_hbm, routes_hbm, scores_hbm, gate_hbm, up_hbm, down_hbm,
-    sgate_hbm, sup_hbm, sdown_hbm,
+    sgate_hbm, sup_hbm, sdown_hbm, order_hbm,
     state_out, back, comb, base_out,
-    tokens_v, mix_gain_v, moe_gain_v, head_gain_v, bound_v, routes_v, scores_v,
+    tokens_v, mix_gain_v, moe_gain_v, head_gain_v, bound_v, routes_v, scores_v, order_v,
     forget_w, query_w, input_w, outgate_w, state_v, mix_w, sgate_w, sup_w, sdown_w,
     gate_own, up_own, down_own, gate_par, up_par, down_par,
     mix_send, mix_recv, shared_send, shared_recv, residual_v,
@@ -130,8 +142,8 @@
         pltpu.make_async_copy(src, dst, load_sem.at[i])
         for i, (src, dst) in enumerate(
             (
-                (tokens_hbm, tokens_v), (mix_gain_hbm, mix_gain_v), (routes_hbm, routes_v), (scores_hbm, scores_v),
-                (bound_hbm, bound_v), (head_gain_hbm, head_gain_v), (moe_gain_hbm, moe_gain_v),
+                (tokens_hbm, tokens_v), (mix_gain_hbm, mix_gain_v), (bound_hbm, bound_v), (routes_hbm, routes_v),
+                (scores_hbm, scores_v), (head_gain_hbm, head_gain_v), (moe_gain_hbm, moe_gain_v), (order_hbm, order_v),
             )
         )
     ]
@@ -152,14 +164,13 @@
         states[-1].start()
     mix_load = pltpu.make_async_copy(mix_out_hbm, mix_w, late_sem.at[0])
     mix_load.start()
-    greet_all(ep, tp)
-
-    for copy in small:
+    peers = Peers(ep)
+    greet_all(ep, tp, peers)
+
+    for copy in small[:2]:
         copy.wait()
-    code, weight = route_tables(routes_v[...], scores_v[...], ep)
     tokens = tokens_v[...].astype(f32)
     normed = rms_scale(tokens, mix_gain_v[...]).astype(bf16)
-    place_rows(code, tp, place)
 
     def project(i, w):
         halves[2 * i].wait()
@@ -168,6 +179,7 @@
         return first + dot(normed[:, 1024:], w[1024:])
 
     forget_pre = project(0, forget_w)
+    small[2].wait()
     bound = bound_v[...]
     forget = bound + (1.0 - bound) / (1.0 + jnp.exp(-forget_pre))
     key = (1.0 - bound) / (1.0 + jnp.exp(forget_pre))
@@ -175,6 +187,23 @@
     seen = forget * query
     input_val = project(2, input_w)
     gate = silu(project(3, outgate_w))
+    heads = [slice(128 * h, 128 * h + 128) for h in range(4)]
+    readout = [
+        jnp.sum(key[:, at] * query[:, at], axis=-1, keepdims=True) * input_val[:, at] for at in heads
+    ]
+    row, block = iota((16, 512), 0), iota((16, 512), 1) // 128
+    for c in range(4):
+        states[c].wait()
+        for h in range(4):
+            tiled = jnp.concatenate([seen[:, heads[h]]] * 4, axis=1)
+            spread = jnp.where(row == block + 4 * c, tiled, 0.0).astype(bf16)
+            readout[h] += dot(spread, state_v[pl.ds(4 * c, 4), h].reshape(512, 128).astype(bf16))
+    for copy in small[3:]:
+        copy.wait()
+    head_gain = head_gain_v[...]
+    gated = jnp.concatenate(
+        [rms_scale(readout[h], head_gain) * gate[:, heads[h]] for h in range(4)], axis=1
+    ).astype(bf16)
     late = [
         pltpu.make_async_copy(src, dst, late_sem.at[1 + i])
         for i, (src, dst) in enumerate(
@@ -186,21 +215,6 @@
     ]
     for copy in late:
         copy.start()
-    heads = [slice(128 * h, 128 * h + 128) for h in range(4)]
-    readout = [
-        jnp.sum(key[:, at] * query[:, at], axis=-1, keepdims=True) * input_val[:, at] for at in heads
-    ]
-    row, block = iota((16, 512), 0), iota((16, 512), 1) // 128
-    for c in range(4):
-        states[c].wait()
-        for h in range(4):
-            tiled = jnp.concatenate([seen[:, heads[h]]] * 4, axis=1)
-            spread = jnp.where(row == block + 4 * c, tiled, 0.0).astype(bf16)
-            readout[h] += dot(spread, state_v[pl.ds(4 * c, 4), h].reshape(512, 128).astype(bf16))
-    head_gain = head_gain_v[...]
-    gated = jnp.concatenate(
-        [rms_scale(readout[h], head_gain) * gate[:, heads[h]] for h in range(4)], axis=1
-    ).astype(bf16)
     mix_load.wait()
     mix_send[...] = dot(gated, mix_w[...]).astype(bf16)
     await_all()
@@ -212,6 +226,8 @@
     ]
     for copy in pushes:
         copy.start()
+    code, weight = route_tables(routes_v[...], scores_v[...], order_v[...], ep)
+    place_rows(code, tp, place)
     mix_copy.wait()
     mixer = (mix_send[...].astype(f32) + mix_recv[...].astype(f32)).astype(bf16)
     residual = tokens + mixer.astype(f32)
@@ -220,22 +236,15 @@
     rows = rms_scale(residual, moe_gain_v[...]).astype(bf16)
     stacked = jnp.concatenate([rows[:, 256 * j : 256 * (j + 1)] for j in range(8)], axis=0)
 
-    def go(i):
-        return pltpu.make_async_remote_copy(
-            src_ref=send.at[i], dst_ref=recv.at[i], send_sem=go_send, recv_sem=go_recv,
-            device_id=(toward(ep, i, 1), tp), device_id_type=MESH,
-        )
-
     for b in range(4):
         placed = dot(place[pl.ds(256 * b, 256), :], stacked).astype(bf16)
         send[pl.ds(16 * b, 16)] = placed.reshape(16, 16, 256)
-
-        def start(i, c):
-            go(i).start()
-            return c
-
-        lax.fori_loop(max(1, 16 * b), 16 * b + 16, start, 0)
-    recv[0] = send[0]
+        for p in range(16 * b, min(16 * b + 16, 63)):
+            pltpu.make_async_remote_copy(
+                src_ref=send.at[p], dst_ref=recv.at[p], send_sem=go_send, recv_sem=go_recv.at[p // 32],
+                device_id=(peers.ahead(p), tp), device_id_type=MESH,
+            ).start()
+    recv[63] = send[63]
 
     for copy in late[:3]:
         copy.wait()
@@ -258,62 +267,54 @@
         return c
 
     lax.fori_loop(0, 4, update, 0)
-    for copy in late[3:]:
-        copy.wait()
-    for copy in pushes:
-        copy.wait()
-    pltpu.make_async_remote_copy(
-        src_ref=all_of(send, 63), dst_ref=all_of(recv, 63), send_sem=go_send, recv_sem=go_recv,
-        device_id=partner, device_id_type=MESH,
-    ).wait()
-
     out_row, in_row = iota((256, 256), 0), iota((256, 256), 1)
     sort = ((out_row // 32 == in_row % 8) & ((out_row // 2) % 16 == in_row // 16)
             & (out_row % 2 == (in_row // 8) % 2)).astype(bf16)
     unsort = ((in_row // 32 == out_row % 8) & ((in_row // 2) % 16 == out_row // 16)
               & (in_row % 2 == (out_row // 8) % 2)).astype(bf16)
-    for b in range(4):
-        sorted_rows = dot(sort, recv[pl.ds(16 * b, 16)].reshape(256, 256)).astype(bf16)
-        for j in range(8):
-            xs[pl.ds(32 * b, 32), pl.ds(256 * j, 256)] = sorted_rows[32 * j : 32 * j + 32]
-    x = xs[...]
-    hidden_own = (silu(dot(x, gate_own[...])) * dot(x, up_own[...])).astype(bf16)
-    hidden_par = (silu(dot(x, gate_par[...])) * dot(x, up_par[...])).astype(bf16)
-    for n in range(8):
-        cols = pl.ds(256 * n, 256)
-        xs[:, cols] = (dot(hidden_own, down_own[:, cols]) + dot(hidden_par, down_par[:, cols])).astype(bf16)
-
-    def come(i, h):
-        return pltpu.make_async_remote_copy(
-            src_ref=ret.at[2 * i + h], dst_ref=back.at[2 * i + tp], send_sem=ret_send, recv_sem=ret_recv,
-            device_id=(toward(ep, i, -1), h), device_id_type=MESH,
-        )
-
-    for b in range(4):
-        tall = jnp.concatenate(
-            [
-                jnp.concatenate(
-                    [xs[pl.ds(32 * b, 32), pl.ds(128 * j + 1024 * h, 128)] for h in range(2)], axis=1
-                )
-                for j in range(8)
-            ],
-            axis=0,
-        )
-        turned = dot(unsort, tall).astype(bf16)
-        for i in range(16):
-            for h in range(2):
-                ret[2 * (16 * b + i) + h] = turned[16 * i : 16 * i + 16, 128 * h : 128 * h + 128]
-
-        def start_back(i, c):
-            for h in range(2):
-                come(i, h).start()
-            return c
-
-        lax.fori_loop(max(1, 16 * b), 16 * b + 16, start_back, 0)
-    to_partner(ret.at[1 - tp], back.at[tp], ret_send, ret_recv).start()
-    back[tp] = ret[tp]
+    for copy in late[3:]:
+        copy.wait()
+    for g in range(2):
+        group = pl.ds(32 * g, 32 - g)
+        to_partner(send.at[group], recv.at[group], go_send, go_recv.at[g]).wait_recv()
+        for b in range(2):
+            sorted_rows = dot(sort, recv[pl.ds(32 * g + 16 * b, 16)].reshape(256, 256)).astype(bf16)
+            for j in range(8):
+                xs[g, pl.ds(32 * b, 32), pl.ds(256 * j, 256)] = sorted_rows[32 * j : 32 * j + 32]
+        x = xs[g]
+        hidden_own = (silu(dot(x, gate_own[...])) * dot(x, up_own[...])).astype(bf16)
+        if g == 0:
+            for copy in pushes:
+                copy.wait()
+        hidden_par = (silu(dot(x, gate_par[...])) * dot(x, up_par[...])).astype(bf16)
+        for n in range(8):
+            cols = pl.ds(256 * n, 256)
+            xs[g, :, cols] = (dot(hidden_own, down_own[:, cols]) + dot(hidden_par, down_par[:, cols])).astype(bf16)
+        for b in range(2):
+            tall = jnp.concatenate(
+                [
+                    jnp.concatenate(
+                        [xs[g, pl.ds(32 * b, 32), pl.ds(128 * j + 1024 * h, 128)] for h in range(2)], axis=1
+                    )
+                    for j in range(8)
+                ],
+                axis=0,
+            )
+            turned = dot(unsort, tall).astype(bf16)
+            for i in range(16):
+                p = 32 * g + 16 * b + i
+                for h in range(2):
+                    ret[2 * p + h] = turned[16 * i : 16 * i + 16, 128 * h : 128 * h + 128]
+                    if p < 63:
+                        pltpu.make_async_remote_copy(
+                            src_ref=ret.at[2 * p + h], dst_ref=back.at[2 * p + tp], send_sem=ret_send,
+                            recv_sem=ret_recv, device_id=(peers.behind(p), h), device_id_type=MESH,
+                        ).start()
+    to_partner(ret.at[127 - tp], back.at[126 + tp], ret_send, ret_recv).start()
+    back[126 + tp] = ret[126 + tp]
     shared_copy.wait()
     base_out[...] = residual_v[tp] + (shared_send[tp].astype(f32) + shared_recv[...].astype(f32)).astype(bf16).astype(f32)
+    to_partner(all_of(send, 63), all_of(recv, 63), go_send, go_recv.at[0]).wait_send()
     to_partner(all_of(ret, 127), all_of(back, 127), ret_send, ret_recv).wait()
 
 
@@ -347,18 +348,18 @@
         out_shape=(
             buf(16, 4, 128, 128, dtype=f32), buf(128, 16, 128), buf(128, 2048), buf(16, 1024, dtype=f32)
         ),
-        in_specs=[hbm] * 19,
+        in_specs=[hbm] * 20,
         out_specs=(vm,) * 4,
         scratch_shapes=[
             buf(16, 2048), buf(1, 2048, dtype=f32), buf(1, 2048, dtype=f32), buf(1, 128, dtype=f32),
-            buf(1, 512, dtype=f32), buf(6, 16, dtype=i32), buf(6, 16, dtype=f32),
+            buf(1, 512, dtype=f32), buf(6, 16, dtype=i32), buf(6, 16, dtype=f32), buf(64, 16, dtype=i32),
             buf(2048, 512), buf(2048, 512), buf(2048, 512), buf(2048, 512), buf(16, 4, 128, 128, dtype=f32),
             buf(512, 2048), buf(2048, 256), buf(2048, 256), buf(256, 2048),
             buf(2048, 256), buf(2048, 256), buf(256, 2048), buf(2048, 256), buf(2048, 256), buf(256, 2048),
             buf(16, 2048), buf(16, 2048), buf(2, 16, 1024), buf(16, 1024), buf(2, 16, 1024, dtype=f32),
             buf(4, 128, 16, dtype=f32), buf(4, 128, 16, dtype=f32), buf(4, 16, 128, dtype=f32),
-            buf(1024, 128), buf(64, 16, 256), buf(64, 16, 256), buf(128, 2048), buf(128, 16, 128),
-            dma((7,)), dma((8,)), dma((4,)), dma((7,)), dma((3,)), dma((3,)), dma((2,)), dma((2,)), dma, dma, dma, dma,
+            buf(1024, 128), buf(64, 16, 256), buf(64, 16, 256), buf(2, 64, 2048), buf(128, 16, 128),
+            dma((8,)), dma((8,)), dma((4,)), dma((7,)), dma((3,)), dma((3,)), dma((2,)), dma((2,)), dma, dma((2,)), dma, dma,
         ],
         compiler_params=pltpu.CompilerParams(
             collective_id=0, has_side_effects=True, vmem_limit_bytes=vmem_all - (5 << 20) - (160 << 10)
@@ -367,6 +368,7 @@
         tokens, state, mix_gain.reshape(1, -1), moe_gain.reshape(1, -1), head_gain.reshape(1, -1),
         w_forget, w_query, w_input, w_outgate, lower_bound.reshape(1, -1), w_mix_out,
         routes.T, route_scores.T, expert_gate, expert_up, expert_down, shared_gate, shared_up, shared_down,
+        jnp.asarray(np.repeat(np.array(order, np.int32)[:, None], 16, 1)),
     )
     return pl.pallas_call(
         finish_kernel,

time: 39.4 us -> 34.7 us (0.88)
  Pallas kernels: 38.7 us -> 33.9 us
    pallas_call x1, Pallas kernels: 36.6 us -> 31.9 us  [local(): pl.pallas_call(layer_kernel, name='layer', out_shape=(buf(16, 4, 128, 128...]
where the time goes in v4:
time: 34.7 us; the launch traced here: 34.5 us
  Pallas kernels  33.9 us (98%)
  between operations  0.65 us (2%)
    pallas_call x1, Pallas kernels, local(): pl.pallas_call(layer_kernel, name='layer', out_shape=(buf(16, 4, 128, 128...  31.9 us
    pallas_call x1, Pallas kernels, local(): pl.pallas_call(finish_kernel, name='finish', out_shape=(jax.ShapeDtypeStr...  2.03 us

profile of v4, /device:TPU:1, one launch (start us, length us, event | category | flops | bytes accessed | tf_op | source)
XLA Modules:
  0.0 34.5 jit_solution(4152893317944003674)
XLA Ops:
  0.6 31.9 %layer.1 = (f32[16,4,128,128]{3,2,1,0:T(8,128)S(1)}, bf16[128,16,128]{2,1,0:T(8,128)(2,1)S(1)}, bf16[128,2048]{1,0:T(8,128)(2,1)S(1)}, f32[16,1024]{1,0:T(8,128)S(1)}) custom-call(bf16[16,2048]{1,0:T(8,128)(2,1)} %tokens_hbm.1, f32[16,4,128,128]{3,2,1,0:T(8,128)} %state_hbm.1, f32[1,2048]{1,0:T(1,128)} %bitcast.6, f32[1,2048]{1,0:T(1,128)} %bitcast.7, ...), custom_call_target="tpu_custom_call" | custom-call | tf_op jit(solution)/shard_map/layer/pallas_call | solution.py:345
  32.5 2.0 %finish.1 = (bf16[16,1024]{1,0:T(8,128)(2,1)}, f32[16,4,128,128]{3,2,1,0:T(8,128)}) custom-call(f32[16,4,128,128]{3,2,1,0:T(8,128)S(1)} %get-tuple-element.6.state_ref, bf16[128,16,128]{2,1,0:T(8,128)(2,1)S(1)} %get-tuple-element.7.back_ref, bf16[128,2048]{1,0:T(8,128)(2,1)S(1)} %get-tuple-element.8.comb_ref, f32[16,1024]{1,0:T(8,128)S(1)} %get-tuple-element.9.base_ref), custom_call_target="tpu_custom_call" | custom-call | tf_op jit(solution)/shard_map/finish/pallas_call | solution.py:373

commit v5 on v4

--- a/solution.py
+++ b/solution.py
@@ -128,7 +128,7 @@
     gate_own, up_own, down_own, gate_par, up_par, down_par,
     mix_send, mix_recv, shared_send, shared_recv, residual_v,
     forget_t, key_t, input_h, place, send, recv, xs, ret,
-    load_sem, half_sem, state_sem, late_sem, push_sem, pull_sem, mix_sems, shared_sems, go_send, go_recv, ret_send, ret_recv,
+    load_sem, half_sem, state_sem, mix_load_sem, late_sem, push_sem, pull_sem, mix_sems, shared_sems, go_send, go_recv, ret_send, ret_recv,
 ):
     ep, tp = lax.axis_index("ep"), lax.axis_index("tp")
     partner = (ep, 1 - tp)
@@ -149,21 +149,30 @@
     ]
     for copy in small:
         copy.start()
-    halves = []
+    big = []
     for i, (src, dst) in enumerate(
-        ((forget_hbm, forget_w), (query_hbm, query_w), (input_hbm, input_w), (outgate_hbm, outgate_w))
+        (
+            (forget_hbm, forget_w), (query_hbm, query_w), (input_hbm, input_w), (outgate_hbm, outgate_w)
+        )
     ):
         for h in range(2):
             rows = pl.ds(1024 * h, 1024)
-            halves.append(pltpu.make_async_copy(src.at[rows], dst.at[rows], half_sem.at[2 * i + h]))
-            halves[-1].start()
-    states = []
+            big.append(pltpu.make_async_copy(src.at[rows], dst.at[rows], half_sem.at[2 * i + h]))
     for c in range(4):
         rows = pl.ds(4 * c, 4)
-        states.append(pltpu.make_async_copy(state_hbm.at[rows], state_v.at[rows], state_sem.at[c]))
-        states[-1].start()
-    mix_load = pltpu.make_async_copy(mix_out_hbm, mix_w, late_sem.at[0])
-    mix_load.start()
+        big.append(pltpu.make_async_copy(state_hbm.at[rows], state_v.at[rows], state_sem.at[c]))
+    for h in range(2):
+        cols = pl.ds(1024 * h, 1024)
+        big.append(pltpu.make_async_copy(mix_out_hbm.at[:, cols], mix_w.at[:, cols], mix_load_sem.at[h]))
+    ahead = 8
+    for copy in big[:ahead]:
+        copy.start()
+
+    def take(i):
+        big[i].wait()
+        if i + ahead < len(big):
+            big[i + ahead].start()
+
     peers = Peers(ep)
     greet_all(ep, tp, peers)
 
@@ -173,9 +182,9 @@
     normed = rms_scale(tokens, mix_gain_v[...]).astype(bf16)
 
     def project(i, w):
-        halves[2 * i].wait()
+        take(2 * i)
         first = dot(normed[:, :1024], w[:1024])
-        halves[2 * i + 1].wait()
+        take(2 * i + 1)
         return first + dot(normed[:, 1024:], w[1024:])
 
     forget_pre = project(0, forget_w)
@@ -193,7 +202,7 @@
     ]
     row, block = iota((16, 512), 0), iota((16, 512), 1) // 128
     for c in range(4):
-        states[c].wait()
+        take(8 + c)
         for h in range(4):
             tiled = jnp.concatenate([seen[:, heads[h]]] * 4, axis=1)
             spread = jnp.where(row == block + 4 * c, tiled, 0.0).astype(bf16)
@@ -204,8 +213,12 @@
     gated = jnp.concatenate(
         [rms_scale(readout[h], head_gain) * gate[:, heads[h]] for h in range(4)], axis=1
     ).astype(bf16)
+    for h in range(2):
+        cols = pl.ds(1024 * h, 1024)
+        take(12 + h)
+        mix_send[:, cols] = dot(gated, mix_w[:, cols]).astype(bf16)
     late = [
-        pltpu.make_async_copy(src, dst, late_sem.at[1 + i])
+        pltpu.make_async_copy(src, dst, late_sem.at[i])
         for i, (src, dst) in enumerate(
             (
                 (sgate_hbm, sgate_w), (sup_hbm, sup_w), (sdown_hbm, sdown_w),
@@ -215,8 +228,6 @@
     ]
     for copy in late:
         copy.start()
-    mix_load.wait()
-    mix_send[...] = dot(gated, mix_w[...]).astype(bf16)
     await_all()
     mix_copy = to_partner(mix_send, mix_recv, mix_sems.at[0], mix_sems.at[1])
     mix_copy.start()
@@ -239,11 +250,11 @@
     for b in range(4):
         placed = dot(place[pl.ds(256 * b, 256), :], stacked).astype(bf16)
         send[pl.ds(16 * b, 16)] = placed.reshape(16, 16, 256)
-        for p in range(16 * b, min(16 * b + 16, 63)):
-            pltpu.make_async_remote_copy(
-                src_ref=send.at[p], dst_ref=recv.at[p], send_sem=go_send, recv_sem=go_recv.at[p // 32],
-                device_id=(peers.ahead(p), tp), device_id_type=MESH,
-            ).start()
+    for p in list(range(16, 63)) + list(range(16)):
+        pltpu.make_async_remote_copy(
+            src_ref=send.at[p], dst_ref=recv.at[p], send_sem=go_send, recv_sem=go_recv.at[int(p >= 16)],
+            device_id=(peers.ahead(p), tp), device_id_type=MESH,
+        ).start()
     recv[63] = send[63]
 
     for copy in late[:3]:
@@ -274,27 +285,28 @@
               & (in_row % 2 == (out_row // 8) % 2)).astype(bf16)
     for copy in late[3:]:
         copy.wait()
-    for g in range(2):
-        group = pl.ds(32 * g, 32 - g)
+    for g, blocks in ((1, range(1, 4)), (0, range(1))):
+        group = pl.ds(16 * blocks[0], 16 * len(blocks) - g)
+        mine = pl.ds(32 * blocks[0], 32 * len(blocks))
         to_partner(send.at[group], recv.at[group], go_send, go_recv.at[g]).wait_recv()
-        for b in range(2):
-            sorted_rows = dot(sort, recv[pl.ds(32 * g + 16 * b, 16)].reshape(256, 256)).astype(bf16)
+        for b in blocks:
+            sorted_rows = dot(sort, recv[pl.ds(16 * b, 16)].reshape(256, 256)).astype(bf16)
             for j in range(8):
-                xs[g, pl.ds(32 * b, 32), pl.ds(256 * j, 256)] = sorted_rows[32 * j : 32 * j + 32]
-        x = xs[g]
+                xs[pl.ds(32 * b, 32), pl.ds(256 * j, 256)] = sorted_rows[32 * j : 32 * j + 32]
+        x = xs[mine, :]
         hidden_own = (silu(dot(x, gate_own[...])) * dot(x, up_own[...])).astype(bf16)
-        if g == 0:
+        if g == 1:
             for copy in pushes:
                 copy.wait()
         hidden_par = (silu(dot(x, gate_par[...])) * dot(x, up_par[...])).astype(bf16)
         for n in range(8):
             cols = pl.ds(256 * n, 256)
-            xs[g, :, cols] = (dot(hidden_own, down_own[:, cols]) + dot(hidden_par, down_par[:, cols])).astype(bf16)
-        for b in range(2):
+            xs[mine, cols] = (dot(hidden_own, down_own[:, cols]) + dot(hidden_par, down_par[:, cols])).astype(bf16)
+        for b in blocks:
             tall = jnp.concatenate(
                 [
                     jnp.concatenate(
-                        [xs[g, pl.ds(32 * b, 32), pl.ds(128 * j + 1024 * h, 128)] for h in range(2)], axis=1
+                        [xs[pl.ds(32 * b, 32), pl.ds(128 * j + 1024 * h, 128)] for h in range(2)], axis=1
                     )
                     for j in range(8)
                 ],
@@ -302,7 +314,7 @@
             )
             turned = dot(unsort, tall).astype(bf16)
             for i in range(16):
-                p = 32 * g + 16 * b + i
+                p = 16 * b + i
                 for h in range(2):
                     ret[2 * p + h] = turned[16 * i : 16 * i + 16, 128 * h : 128 * h + 128]
                     if p < 63:
@@ -358,8 +370,8 @@
             buf(2048, 256), buf(2048, 256), buf(256, 2048), buf(2048, 256), buf(2048, 256), buf(256, 2048),
             buf(16, 2048), buf(16, 2048), buf(2, 16, 1024), buf(16, 1024), buf(2, 16, 1024, dtype=f32),
             buf(4, 128, 16, dtype=f32), buf(4, 128, 16, dtype=f32), buf(4, 16, 128, dtype=f32),
-            buf(1024, 128), buf(64, 16, 256), buf(64, 16, 256), buf(2, 64, 2048), buf(128, 16, 128),
-            dma((8,)), dma((8,)), dma((4,)), dma((7,)), dma((3,)), dma((3,)), dma((2,)), dma((2,)), dma, dma((2,)), dma, dma,
+            buf(1024, 128), buf(64, 16, 256), buf(64, 16, 256), buf(128, 2048), buf(128, 16, 128),
+            dma((8,)), dma((8,)), dma((4,)), dma((2,)), dma((6,)), dma((3,)), dma((3,)), dma((2,)), dma((2,)), dma, dma((2,)), dma, dma,
         ],
         compiler_params=pltpu.CompilerParams(
             collective_id=0, has_side_effects=True, vmem_limit_bytes=vmem_all - (5 << 20) - (160 << 10)

time: 34.7 us -> 34.1 us (0.983)
  Pallas kernels: 33.9 us -> 33.3 us
    pallas_call x1, Pallas kernels: 31.9 us -> 31.3 us  [local(): pl.pallas_call(layer_kernel, name='layer', out_shape=(buf(16, 4, 128, 128...]
where the time goes in v5:
time: 34.1 us; the launch traced here: 34 us
  Pallas kernels  33.3 us (98%)
  between operations  0.65 us (2%)
    pallas_call x1, Pallas kernels, local(): pl.pallas_call(layer_kernel, name='layer', out_shape=(buf(16, 4, 128, 128...  31.3 us
    pallas_call x1, Pallas kernels, local(): pl.pallas_call(finish_kernel, name='finish', out_shape=(jax.ShapeDtypeStr...  2.03 us

profile of v5, /device:TPU:1, one launch (start us, length us, event | category | flops | bytes accessed | tf_op | source)
XLA Modules:
  0.0 34.0 jit_solution(2988399673259126383)
XLA Ops:
  0.6 31.3 %layer.1 = (f32[16,4,128,128]{3,2,1,0:T(8,128)S(1)}, bf16[128,16,128]{2,1,0:T(8,128)(2,1)S(1)}, bf16[128,2048]{1,0:T(8,128)(2,1)S(1)}, f32[16,1024]{1,0:T(8,128)S(1)}) custom-call(bf16[16,2048]{1,0:T(8,128)(2,1)} %tokens_hbm.1, f32[16,4,128,128]{3,2,1,0:T(8,128)} %state_hbm.1, f32[1,2048]{1,0:T(1,128)} %bitcast.6, f32[1,2048]{1,0:T(1,128)} %bitcast.7, ...), custom_call_target="tpu_custom_call" | custom-call | tf_op jit(solution)/shard_map/layer/pallas_call | solution.py:357
  31.9 2.0 %finish.1 = (bf16[16,1024]{1,0:T(8,128)(2,1)}, f32[16,4,128,128]{3,2,1,0:T(8,128)}) custom-call(f32[16,4,128,128]{3,2,1,0:T(8,128)S(1)} %get-tuple-element.6.state_ref, bf16[128,16,128]{2,1,0:T(8,128)(2,1)S(1)} %get-tuple-element.7.back_ref, bf16[128,2048]{1,0:T(8,128)(2,1)S(1)} %get-tuple-element.8.comb_ref, f32[16,1024]{1,0:T(8,128)S(1)} %get-tuple-element.9.base_ref), custom_call_target="tpu_custom_call" | custom-call | tf_op jit(solution)/shard_map/finish/pallas_call | solution.py:385

commit v6 on v5

--- a/solution.py
+++ b/solution.py
@@ -37,7 +37,11 @@
     return sum(min(d, 4 - d) for d in parts(off))
 
 
-order = sorted(range(64), key=lambda off: (-hops(off), off * 37 % 64))
+def turns(off):
+    return sum(d > 0 for d in parts(off))
+
+
+order = sorted(range(64), key=lambda off: (-hops(off), -turns(off), off * 37 % 64))
 
 
 class Peers:

time: 34.1 us -> 34.1 us (level)
  no operation moved by 1% of the time
where the time goes in v6:
time: 34.1 us; the launch traced here: 34 us
  Pallas kernels  33.3 us (98%)
  between operations  0.65 us (2%)
    pallas_call x1, Pallas kernels, local(): pl.pallas_call(layer_kernel, name='layer', out_shape=(buf(16, 4, 128, 128...  31.3 us
    pallas_call x1, Pallas kernels, local(): pl.pallas_call(finish_kernel, name='finish', out_shape=(jax.ShapeDtypeStr...  2.03 us

profile of v6, /device:TPU:1, one launch (start us, length us, event | category | flops | bytes accessed | tf_op | source)
XLA Modules:
  0.0 34.0 jit_solution(5822328824737455407)
XLA Ops:
  0.6 31.3 %layer.1 = (f32[16,4,128,128]{3,2,1,0:T(8,128)S(1)}, bf16[128,16,128]{2,1,0:T(8,128)(2,1)S(1)}, bf16[128,2048]{1,0:T(8,128)(2,1)S(1)}, f32[16,1024]{1,0:T(8,128)S(1)}) custom-call(bf16[16,2048]{1,0:T(8,128)(2,1)} %tokens_hbm.1, f32[16,4,128,128]{3,2,1,0:T(8,128)} %state_hbm.1, f32[1,2048]{1,0:T(1,128)} %bitcast.6, f32[1,2048]{1,0:T(1,128)} %bitcast.7, ...), custom_call_target="tpu_custom_call" | custom-call | tf_op jit(solution)/shard_map/layer/pallas_call | solution.py:361
  31.9 2.0 %finish.1 = (bf16[16,1024]{1,0:T(8,128)(2,1)}, f32[16,4,128,128]{3,2,1,0:T(8,128)}) custom-call(f32[16,4,128,128]{3,2,1,0:T(8,128)S(1)} %get-tuple-element.6.state_ref, bf16[128,16,128]{2,1,0:T(8,128)(2,1)S(1)} %get-tuple-element.7.back_ref, bf16[128,2048]{1,0:T(8,128)(2,1)S(1)} %get-tuple-element.8.comb_ref, f32[16,1024]{1,0:T(8,128)S(1)} %get-tuple-element.9.base_ref), custom_call_target="tpu_custom_call" | custom-call | tf_op jit(solution)/shard_map/finish/pallas_call | solution.py:389
